TPU v7x, 32 devices: a whole 2x2x4 slice. The times are simulated.
32 devices in a mesh: sp: 8 (over z, x), tp: 4 (over y, core).
Axes of the slice: x: 2, y: 2, z: 4, core: 2. Of those that a mesh axis runs over, the one named last changes fastest.
Arguments:
- resid: bfloat16 [4096, 2048], P(('sp', 'tp')), may hold values from -6 to 6
- pool_in: bfloat16 [4096, 1024], P('sp', 'tp'), may hold values from -8 to 8
- doc_ids: int32 [4096], P('sp'), may hold values from 0 to 3, never falling along the last dimension, each value on 1 to 1536 neighbouring positions
- w_group: bfloat16 [8, 128, 128], replicated, may hold values from -0.5 to 0.5
- pool_scale: bfloat16 [1024], replicated, may hold values from 0.099609375 to 1.8984375
- w_branch: bfloat16 [1024, 2048], P('tp'), may hold values from -0.1875 to 0.1875
- norm_gain: bfloat16 [2048], replicated, may hold values from 0.099609375 to 1.8984375
- route_ids: int32 [4096, 4], P(('sp', 'tp')), may hold values from 0 to 31, all different within a row; in each aligned block of 128 rows (0 to 127, 128 to 255, ...) at most 32 rows name the same one
- route_wts: float32 [4096, 4], P(('sp', 'tp')), may hold values from 0.2 to 1
- w_exp_gate: bfloat16 [32, 2048, 512], P(('sp', 'tp')), may hold values from -0.125 to 0.125
- w_exp_up: bfloat16 [32, 2048, 512], P(('sp', 'tp')), may hold values from -0.125 to 0.125
- w_exp_down: bfloat16 [32, 512, 2048], P(('sp', 'tp')), may hold values from -0.25 to 0.25
- w_sh_gate: bfloat16 [2048, 512], replicated, may hold values from -0.125 to 0.125
- w_sh_up: bfloat16 [2048, 512], replicated, may hold values from -0.125 to 0.125
- w_sh_down: bfloat16 [512, 2048], replicated, may hold values from -0.25 to 0.25
- final_gain: bfloat16 [2048], replicated, may hold values from 0.099609375 to 1.8984375
Outputs:
- final: bfloat16 [4096, 2048], P(('sp', 'tp'))
Inputs may be any that keep to these rules, and one draw needn't show every extreme that they name: `doc_ids`: never falls along the positions. `route_ids`: each row names 4 different experts; among the rows of one device (aligned blocks of 128 rows) no expert is named by more than 32 rows, a bound that some block reaches.
All inputs are finite; a program needn't handle non-finite values.
Results may differ from a plain program's by a relative error of at most 0.0062.
Values may be sent and summed in bfloat16 or wider, within the bound.
No kernel may reach another device: no remote copies, remote signals or barrier semaphores. Data moves between devices by JAX's collectives and lax.ppermute only.
A program may use at most 128 MiB of HBM per device.

v0:
```python
import jax
import jax.numpy as jnp
from jax import lax
from jax.sharding import PartitionSpec as P

pool_windows = (2, 4, 8, 16, 16, 32, 64, 128)
alpha_mix = 8.0**0.25
norm_eps = 1e-05


def carried_in(value, axis, combine, identity):
    length, here = (lax.axis_size(axis), lax.axis_index(axis))
    everything = jax.tree.map(lambda part: lax.all_gather(part, axis), value)
    start = jax.tree.map(
        lambda part, zero: jnp.broadcast_to(jnp.asarray(zero, part.dtype), part.shape),
        value,
        identity,
    )

    def lap(k, before):
        reached = k < here
        new = combine(before, jax.tree.map(lambda part: part[k], everything))
        return jax.tree.map(lambda a, b: jnp.where(reached, a, b), new, before)

    return lax.fori_loop(0, length, lap, start)


def shifted(value, axis, by):
    length = lax.axis_size(axis)
    pairs = [(i, i + by) for i in range(length) if 0 <= i + by < length]
    return lax.ppermute(value, axis, pairs)


def layer_norm(values, scales):
    center = values - jnp.mean(values, axis=-1, keepdims=True)
    spread = jnp.mean(center * center, axis=-1, keepdims=True)
    return center * lax.rsqrt(spread + norm_eps) * scales.astype(jnp.float32)


def channel_windows(first_channel, channel_count, group_width):
    groups = (first_channel + jnp.arange(channel_count, dtype=jnp.int32)) // group_width
    window_table = jnp.asarray(pool_windows, dtype=jnp.int32)
    matches = groups[:, None] == jnp.arange(len(pool_windows), dtype=jnp.int32)[None, :]
    return jnp.sum(jnp.where(matches, window_table[None, :], 0), axis=1).astype(jnp.float32)


def swiglu_hidden(token_rows, gate_weight, up_weight):
    gate_vals = jnp.dot(token_rows, gate_weight, preferred_element_type=jnp.float32)
    up_vals = jnp.dot(token_rows, up_weight, preferred_element_type=jnp.float32)
    return (jax.nn.silu(gate_vals) * up_vals).astype(jnp.bfloat16)


def join_prefix(earlier, later):
    early_doc, early_count, early_sums = earlier
    late_doc, late_count, late_sums = later
    is_empty = late_count == 0.0
    same_doc = late_doc == early_doc
    new_doc = jnp.where(is_empty, early_doc, late_doc)
    new_count = jnp.where(
        is_empty, early_count, jnp.where(same_doc, early_count + late_count, late_count)
    )
    new_sums = jnp.where(
        is_empty, early_sums, jnp.where(same_doc, early_sums + late_sums, late_sums)
    )
    return (new_doc, new_count, new_sums)


def local(
    resid,
    pool_in,
    doc_ids,
    w_group,
    pool_scale,
    w_branch,
    norm_gain,
    route_ids,
    route_wts,
    w_exp_gate,
    w_exp_up,
    w_exp_down,
    w_sh_gate,
    w_sh_up,
    w_sh_down,
    final_gain,
):
    tok_count, local_width = pool_in.shape
    group_width = w_group.shape[1]
    halo_rows = max(pool_windows) - 1
    channel_first = lax.axis_index("tp") * local_width
    values = pool_in.astype(jnp.float32)
    positions = jnp.arange(tok_count, dtype=jnp.int32)
    last_doc = doc_ids[-1]
    change = jnp.concatenate([jnp.ones((1,), bool), doc_ids[1:] != doc_ids[:-1]])
    doc_start = lax.cummax(jnp.where(change, positions, 0), axis=0)
    trailing = doc_ids == last_doc
    tail_sums = jnp.sum(jnp.where(trailing[:, None], values, 0.0), axis=0)
    tail_count = jnp.sum(trailing.astype(jnp.float32)).reshape(1)
    tail_doc = last_doc.astype(jnp.float32).reshape(1)
    identity = (
        jnp.full((1,), -1.0, jnp.float32),
        jnp.zeros((1,), jnp.float32),
        jnp.zeros((local_width,), jnp.float32),
    )
    prev_doc, prev_count, prev_sums = carried_in(
        (tail_doc, tail_count, tail_sums), "sp", join_prefix, identity
    )
    before = shifted(pool_in[tok_count - halo_rows :], "sp", 1)
    extended = jnp.concatenate([before, pool_in], axis=0).astype(jnp.float32)
    cumulative = jnp.concatenate(
        [jnp.zeros((1, local_width), jnp.float32), jnp.cumsum(extended, axis=0)], axis=0
    )
    current = cumulative[halo_rows + 1 :]
    local_cum = current - cumulative[halo_rows]
    local_zero = jnp.concatenate([jnp.zeros((1, local_width), jnp.float32), local_cum], axis=0)
    carried = doc_ids.astype(jnp.float32) == prev_doc
    running = (
        local_cum - local_zero[doc_start] + jnp.where(carried[:, None], prev_sums[None, :], 0.0)
    )
    since_start = (positions - doc_start).astype(jnp.float32) + jnp.where(carried, prev_count, 0.0)
    since_start = since_start[:, None]
    doc_mean = running / (since_start + 1.0)
    widths = channel_windows(channel_first, local_width, group_width)[None, :]
    recent = running
    for window in sorted(set(pool_windows)):
        lagged = cumulative[halo_rows + 1 - window : halo_rows + 1 - window + tok_count]
        recent = jnp.where((widths == window) & (since_start >= window), current - lagged, recent)
    window_mean = recent / jnp.minimum(since_start + 1.0, widths)
    offset = (0.5 * (window_mean + doc_mean) - values).astype(jnp.bfloat16)
    group_count = local_width // group_width
    local_groups = lax.dynamic_slice_in_dim(
        w_group, lax.axis_index("tp") * group_count, group_count, 0
    )
    mixed_rows = jnp.einsum(
        "tgc,gcd->tgd",
        offset.reshape(tok_count, group_count, group_width),
        local_groups,
        preferred_element_type=jnp.float32,
    ).reshape(tok_count, local_width)
    scale_local = lax.dynamic_slice_in_dim(pool_scale, channel_first, local_width, 0).astype(
        jnp.float32
    )
    mixed_rows = (mixed_rows * scale_local[None, :]).astype(jnp.bfloat16)
    row_count, model_width = resid.shape
    token_rows = lax.all_to_all(mixed_rows, "tp", split_axis=0, concat_axis=1, tiled=True)
    branch = jnp.dot(
        token_rows,
        lax.all_gather(w_branch, "tp", axis=0, tiled=True),
        preferred_element_type=jnp.float32,
    )
    normed = layer_norm(alpha_mix * resid.astype(jnp.float32) + branch, norm_gain).astype(
        jnp.bfloat16
    )
    top_count = route_ids.shape[1]
    expert_total = lax.axis_size("sp") * lax.axis_size("tp")
    capacity = 2 * row_count * top_count // expert_total
    flat_ids = route_ids.reshape(-1)
    onehot = (flat_ids[:, None] == jnp.arange(expert_total, dtype=jnp.int32)[None, :]).astype(
        jnp.int32
    )
    slot_rank = jnp.sum(jnp.cumsum(onehot, axis=0) * onehot, axis=1) - 1
    slot_index = flat_ids * capacity + slot_rank
    assign_total = row_count * top_count
    source = jnp.full((expert_total * capacity,), assign_total, jnp.int32)
    source = source.at[slot_index].set(jnp.arange(assign_total, dtype=jnp.int32))
    padded = jnp.concatenate([normed, jnp.zeros((1, model_width), jnp.bfloat16)], axis=0)
    outgoing = padded[source // top_count].reshape(expert_total, capacity, model_width)
    arrived = lax.all_to_all(outgoing, ("sp", "tp"), split_axis=0, concat_axis=0, tiled=True)
    flat_rows = arrived.reshape(-1, model_width)
    hidden = swiglu_hidden(flat_rows, w_exp_gate[0], w_exp_up[0])
    expert_out = jnp.dot(hidden, w_exp_down[0], preferred_element_type=jnp.float32).astype(
        jnp.bfloat16
    )
    returned = lax.all_to_all(
        expert_out.reshape(arrived.shape), ("sp", "tp"), split_axis=0, concat_axis=0, tiled=True
    )
    returned = returned.reshape(expert_total * capacity, model_width)
    picked = returned[slot_index].astype(jnp.float32).reshape(row_count, top_count, model_width)
    routed = jnp.sum(picked * route_wts[:, :, None], axis=1)
    shared = jnp.dot(
        swiglu_hidden(normed, w_sh_gate, w_sh_up), w_sh_down, preferred_element_type=jnp.float32
    )
    return layer_norm(alpha_mix * normed.astype(jnp.float32) + routed + shared, final_gain).astype(
        jnp.bfloat16
    )


def solution(mesh):
    placed = (
        P(("sp", "tp"), None),
        P("sp", "tp"),
        P("sp"),
        P(),
        P(),
        P("tp", None),
        P(),
        P(("sp", "tp"), None),
        P(("sp", "tp"), None),
        P(("sp", "tp"), None, None),
        P(("sp", "tp"), None, None),
        P(("sp", "tp"), None, None),
        P(),
        P(),
        P(),
        P(),
    )
    return jax.shard_map(
        local, mesh=mesh, in_specs=placed, out_specs=P(("sp", "tp"), None), check_vma=False
    )
```

profile of v0, /device:TPU:0, one launch (start us, length us, event | category | flops | bytes accessed | tf_op | source)
XLA Modules:
  0.0 369.8 jit_solution(11847515361209987746)
XLA Ops:
  6.6 1.0 slice.74
  7.6 4.9 %collective-permute-start = (bf16[127,256]{1,0:T(8,128)(2,1)S(1)}, bf16[127,256]{1,0:T(8,128)(2,1)S(1)}, u32[]{:S(2)}, u32[]{:S(2)}) collective-permute-start(bf16[127,256]{1,0:T(8,128)(2,1)S(1)} %slice.74), channel_id=1, source_target_pairs={{0,4},{4,8},{8,12},{12,16},{16,20},{20,24},{24,28},{1,5},{5,9},{9,... | collective-permute-start | bytes 195080 | tf_op jit(solution)/shard_map/ppermute | solution.py:31
  12.5 1.3 slice.73
  13.8 1.9 convert_reduce_fusion
  16.4 0.8 slice_compare_fusion
  17.2 0.8 copy.48
  18.2 0.7 broadcast_multiply_fusion
  18.9 1.1 fusion.17
  20.0 18.7 %all-gather.1 = f32[8,1,256]{2,1,0:T(1,128)S(1)} all-gather(f32[1,1,256]{2,1,0:T(1,128)S(1)} %bitcast.132), channel_id=2, replica_groups=mesh['sp'=8,'tp'=4] {'sp'}, dimensions={0}, use_global_device_ids=true | all-gather | bytes 9216 | tf_op jit(solution)/shard_map/all_gather | solution.py:13
  38.8 0.3 reduce-window.21
  39.2 0.7 select_reduce_fusion
  39.9 0.6 convert_element_type.94
  40.5 0.7 convert_element_type.103
  41.2 1.2 reduce-window.29
  42.4 0.2 slice_reduce_fusion
  42.8 0.1 copy.47
  42.9 0.6 dynamic-slice
  43.5 1.3 dynamic-update-slice
  44.8 0.7 dynamic-update-slice.1
  45.6 17.1 %all-reduce.6 = (f32[8]{0:T(128)S(1)}, f32[8]{0:T(128)S(1)}) all-reduce(f32[8]{0:T(128)S(1)} %dynamic-update-slice, f32[8]{0:T(128)S(1)} %dynamic-update-slice.1), channel_id=1, replica_groups=mesh['sp'=8,'tp'=4] {'sp'}, use_global_device_ids=true, to_apply=%add.4 | all-reduce | flops 16 | bytes 128
  62.8 3.0 scatter_custom_fusion
  65.8 0.1 slice_reduce_fusion.1
  65.9 28.7 %while.18 = (s32[]{:T(128)}, f32[1]{0:T(128)}, f32[1]{0:T(128)}, f32[256]{0:T(256)S(1)}, s32[]{:T(128)}, /*index=5*/f32[8,1]{0,1:T(1,128)S(1)}, f32[8,1]{0,1:T(1...) while((s32[]{:T(128)}, f32[1]{0:T(128)}, f32[1]{0:T(128)}, ...), condition=%wide.region_6.7_spmd.clone, body=%wide.region_5.6_spmd.clone.sunk | while | flops 1292 | bytes 5370 | solution.py:25
  65.9 0.6 constant_dynamic-slice_fusion.5
  69.5 0.6 constant_dynamic-slice_fusion.5
  73.1 0.6 constant_dynamic-slice_fusion.5
  76.7 0.6 constant_dynamic-slice_fusion.5
  80.3 0.6 constant_dynamic-slice_fusion.5
  83.9 0.6 constant_dynamic-slice_fusion.5
  87.4 0.6 constant_dynamic-slice_fusion.5
  91.0 0.6 constant_dynamic-slice_fusion.5
  94.6 0.6 broadcast_compare_fusion.6
  95.3 0.6 pad_clamp_fusion.1
  95.9 0.6 broadcast_add_fusion.2
  96.4 0.6 broadcast_compare_fusion.14
  97.1 0.6 broadcast_compare_fusion.5
  97.7 1.3 dynamic-slice_convert_fusion
  99.2 0.7 fusion.8
  100.0 0.2 copy.44
  100.2 0.5 copy-done.10
  100.8 2.4 gather_fusion
  103.2 3.6 convolution_bitcast_fusion
  106.8 1.3 reshape.240
  108.1 1.5 fusion.24
  109.6 3.4 all-to-all-start
  113.0 5.9 %all-to-all-done = bf16[4,128,256]{1,2,0:T(8,128)(2,1)S(1)} async-done(((bf16[4,128,256]{1,2,0:T(8,128)(2,1)}), bf16[4,128,256]{1,2,0:T(8,128)(2,1)S(1)}, u32[]{:S(2)}, u32[]{:S(2)}) %all-to-all-start) | async-done | bytes 262176 | tf_op jit(solution)/shard_map/all_to_all | solution.py:144
  118.9 3.0 fusion.50
  122.0 0.3 multiply_reduce_fusion.2
  122.2 0.2 multiply_convert_fusion.2
  122.5 6.0 %gather_fusion.1 = bf16[1024,2048]{1,0:T(8,128)(2,1)} fusion(bf16[129,2048]{1,0:T(8,128)(2,1)S(1)} %concatenate.22, s32[1024]{0:T(1024)S(1)} %fusion.40), kind=kCustom, calls=%fused_computation.1 | custom fusion | bytes 8392704 | tf_op jit(solution)/shard_map/gather | solution.py:166
  128.5 96.5 %all_to_all.26 = bf16[32,32,2048]{2,1,0:T(8,128)(2,1)S(1)} all-to-all(bf16[32,32,2048]{2,1,0:T(8,128)(2,1)} %bitcast.112), channel_id=1, replica_groups=mesh['sp'=8,'tp'=4] {'sp','tp'}, dimensions={0} | all-to-all | bytes 8388608 | tf_op jit(solution)/shard_map/all_to_all | solution.py:167
  225.1 2.0 copy-done.2
  227.0 3.7 %fusion.1 = f32[1024,512]{1,0:T(8,128)} fusion(bf16[1024,2048]{1,0:T(8,128)(2,1)S(1)} %bitcast.114, bf16[1,2048,512]{2,1,0:T(8,128)(2,1)S(1)} %copy-done.13), kind=kOutput, calls=%fused_computation.14 | convolution fusion | flops 2147483648 | bytes 8388608 | tf_op jit(solution)/shard_map/dot_general | solution.py:49
  230.8 10.1 %convolution_convert_fusion = bf16[1024,2048]{1,0:T(8,128)(2,1)} fusion(bf16[1,512,2048]{2,1,0:T(8,128)(2,1)S(1)} %copy-done, f32[1024,512]{1,0:T(8,128)} %fusion.1, bf16[1024,2048]{1,0:T(8,128)(2,1)} %bitcast.115, bf16[1,2048,512]{2,1,0:T(8,128)(2,1)} %param.28), kind=kOutput, calls=%fused_computation.10 | convolution fusion | flops 4300210176 | bytes 14680064 | tf_op jit(solution)/shard_map/dot_general | solution.py:170
  240.8 3.9 %all-to-all-start.2 = ((bf16[32,32,2048]{2,1,0:T(8,128)(2,1)}), bf16[32,32,2048]{2,1,0:T(8,128)(2,1)}, u32[]{:S(2)}, u32[]{:S(2)}) async-start(bf16[32,32,2048]{2,1,0:T(8,128)(2,1)} %bitcast.113), calls=%async_computation.2 | async-start | bytes 8388608 | tf_op jit(solution)/shard_map/all_to_all | solution.py:173
  244.8 0.1 copy.51
  244.9 2.0 fusion.52
  247.0 91.8 %all-to-all-done.2 = bf16[32,32,2048]{2,1,0:T(8,128)(2,1)} async-done(((bf16[32,32,2048]{2,1,0:T(8,128)(2,1)}), bf16[32,32,2048]{2,1,0:T(8,128)(2,1)}, u32[]{:S(2)}, u32[]{:S(2)}) %all-to-all-start.2) | async-done | bytes 4194336 | tf_op jit(solution)/shard_map/all_to_all | solution.py:173
  338.8 8.0 %gather_fusion.2 = bf16[512,2048]{1,0:T(8,128)(2,1)} fusion(bf16[1024,2048]{1,0:T(8,128)(2,1)} %bitcast.32, s32[1024]{0:T(1024)S(1)} %pad_clamp_fusion), kind=kCustom, calls=%fused_computation.2 | custom fusion | bytes 4196352 | tf_op jit(solution)/shard_map/gather | solution.py:177
  346.8 4.8 %reshape.247 = f32[128,4,2048]{2,1,0:T(4,128)} reshape(bf16[512,2048]{1,0:T(8,128)(2,1)} %gather_fusion.2) | data formatting | bytes 6291456 | tf_op jit(solution)/shard_map/convert_element_type | solution.py:177
  351.5 6.3 %multiply_reduce_fusion = f32[128,2048]{1,0:T(8,128)} fusion(f32[128,4,2048]{2,1,0:T(4,128)} %reshape.247, f32[128,4]{1,0:T(8,128)S(1)} %copy.51), kind=kLoop, calls=%fused_computation.9 | loop fusion | flops 1835008 | bytes 5244928 | tf_op jit(solution)/shard_map/reduce_sum | solution.py:178
  357.9 3.8 %fusion.51 = (f32[128]{0:T(128)S(1)}, f32[128,2048]{1,0:T(8,128)S(1)}) fusion(bf16[512,2048]{1,0:T(8,128)(2,1)} %param.33, bf16[128,2048]{1,0:T(8,128)(2,1)} %copy-done.1, bf16[2048,512]{1,0:T(8,128)(2,1)} %param.32, f32[128,512]{1,0:T(8,128)S(1)} %fusion.52, f32[128,2048]{1,0:T(8,128)} %multiply_reduce_fusion), kind=kOutput, calls=%fused_computation.133 | convolution fusion | flops 538574720 | bytes 7078400 | tf_op jit(solution)/shard_map/dot_general | solution.py:179
  361.7 0.3 multiply_reduce_fusion.1
  361.9 1.0 multiply_convert_fusion.1
  (84 shorter events, 1.4 us)
Async XLA Ops:
  6.5 224.2 %copy-start = (bf16[1,512,2048]{2,1,0:T(8,128)(2,1)S(1)}, bf16[1,512,2048]{2,1,0:T(8,128)(2,1)}, u32[]{:S(2)}) copy-start(bf16[1,512,2048]{2,1,0:T(8,128)(2,1)} %param.30) | copy-start | bytes 6291460
  6.5 36.3 %copy-start.14 = (u32[32]{0:T(128)S(1)}, u32[32]{0:T(128)}, u32[]{:S(2)}) copy-start(u32[32]{0:T(128)} %constant.167) | copy-start | bytes 388
  6.5 92.5 %copy-start.3 = (bf16[512,256]{1,0:T(8,128)(2,1)S(1)}, bf16[512,256]{1,0:T(8,128)(2,1)}, u32[]{:S(2)}) copy-start(bf16[512,256]{1,0:T(8,128)(2,1)} %param.20) | copy-start | bytes 786436
  6.5 88.1 %copy-start.5 = (s32[512]{0:T(512)S(1)}, s32[512]{0:T(512)}, u32[]{:S(2)}) copy-start(s32[512]{0:T(512)} %param.21) | copy-start | bytes 6148
  6.5 112.4 %all-gather.4.cloned.1.call-start = ((), (), s32[]{:S(2)}) async-start(), calls=%async_computation.3 | async-start | bytes 5242880 | tf_op jit(solution)/shard_map/all_gather | solution.py:147
  7.6 91.4 %collective-permute-start = (bf16[127,256]{1,0:T(8,128)(2,1)S(1)}, bf16[127,256]{1,0:T(8,128)(2,1)S(1)}, u32[]{:S(2)}, u32[]{:S(2)}) collective-permute-start(bf16[127,256]{1,0:T(8,128)(2,1)S(1)} %slice.74), channel_id=1, source_target_pairs={{0,4},{4,8},{8,12},{12,16},{16,20},{20,24},{24,28},{1,5},{5,9},{9,... | collective-permute-start | bytes 195080 | tf_op jit(solution)/shard_map/ppermute | solution.py:31
  62.8 3.1 copy-start.8
  94.6 4.5 %copy-start.6 = (f32[256]{0:T(256)}, f32[256]{0:T(256)S(1)}, u32[]{:S(2)}) copy-start(f32[256]{0:T(256)S(1)} %get-tuple-element.148) | copy-start | bytes 3076
  100.2 0.5 copy-start.10
  106.8 6.2 %copy-start.7 = (s32[1024]{0:T(1024)S(1)}, s32[1024]{0:T(1024)}, u32[]{:S(2)}) copy-start(s32[1024]{0:T(1024)} %scatter_custom_fusion) | copy-start | bytes 12292
  106.8 12.1 %copy-start.4 = (bf16[128,2048]{1,0:T(8,128)(2,1)S(1)}, bf16[128,2048]{1,0:T(8,128)(2,1)}, u32[]{:S(2)}) copy-start(bf16[128,2048]{1,0:T(8,128)(2,1)} %param.19) | copy-start | bytes 1572868
  109.6 9.4 %all-to-all-start = ((bf16[4,128,256]{1,2,0:T(8,128)(2,1)}), bf16[4,128,256]{1,2,0:T(8,128)(2,1)S(1)}, u32[]{:S(2)}, u32[]{:S(2)}) async-start(bf16[4,128,256]{1,2,0:T(8,128)(2,1)} %fusion.24), calls=%async_computation | async-start | bytes 524288 | tf_op jit(solution)/shard_map/all_to_all | solution.py:144
  122.5 122.5 %copy-start.1 = (bf16[128,2048]{1,0:T(8,128)(2,1)}, bf16[128,2048]{1,0:T(8,128)(2,1)S(1)}, u32[]{:S(2)}) copy-start(bf16[128,2048]{1,0:T(8,128)(2,1)S(1)} %multiply_convert_fusion.2) | copy-start | bytes 1572868
  128.5 98.5 %copy-start.13 = (bf16[1,2048,512]{2,1,0:T(8,128)(2,1)S(1)}, bf16[1,2048,512]{2,1,0:T(8,128)(2,1)}, u32[]{:S(2)}) copy-start(bf16[1,2048,512]{2,1,0:T(8,128)(2,1)} %param.29) | copy-start | bytes 6291460
  225.1 2.0 copy-start.2
  240.8 4.0 %copy-start.12 = (f32[128,4]{0,1:T(4,128)S(1)}, f32[128,4]{0,1:T(4,128)}, u32[]{:S(2)}) copy-start(f32[128,4]{0,1:T(4,128)} %param.27) | copy-start | bytes 6148
  240.8 4.1 %copy-start.11 = (bf16[2048]{0:T(1024)(128)(2,1)S(1)}, bf16[2048]{0:T(1024)(128)(2,1)}, u32[]{:S(2)}) copy-start(bf16[2048]{0:T(1024)(128)(2,1)} %param.34) | copy-start | bytes 12292
  240.8 4.1 %copy-start.9 = (s32[512,1]{0,1:T(1,128)S(1)}, s32[512,1]{0,1:T(1,128)}, u32[]{:S(2)}) copy-start(s32[512,1]{0,1:T(1,128)} %copy-done.8) | copy-start | bytes 6148
  240.8 98.0 %all-to-all-start.2 = ((bf16[32,32,2048]{2,1,0:T(8,128)(2,1)}), bf16[32,32,2048]{2,1,0:T(8,128)(2,1)}, u32[]{:S(2)}, u32[]{:S(2)}) async-start(bf16[32,32,2048]{2,1,0:T(8,128)(2,1)} %bitcast.113), calls=%async_computation.2 | async-start | bytes 8388608 | tf_op jit(solution)/shard_map/all_to_all | solution.py:173
Sparse Core Ops, SparseCore 0:
  12.6 34.7 all-gather.3
where the time goes:
time: 371 us; the launch traced here: 370 us
  blocking collectives  132 us (36%)
  waiting for transfers between devices  97.8 us (26%)
  local copies, waits for them, and re-layouts  39.7 us (11%)
  matrix products  26.2 us (7%)
  loops' own time  23.8 us (6%)
  other arithmetic  23.3 us (6%)
  between operations  14.4 us (4%)
  starting transfers between devices  12.3 us (3%)
    all_to_all x1, blocking collectives, local(): lax.all_to_all(outgoing, ('sp', 'tp'), split_axis=0, concat_axis=0, tiled...  96.5 us
    all_to_all x1, waiting for transfers between devices, local(): lax.all_to_all(expert_out.reshape(arrived.shape), ('sp', 'tp'), split_axi...  91.8 us
    another operation x1, loops' own time, carried_in(): return lax.fori_loop(0, length, lap, start)  23.8 us
    all_gather x1, blocking collectives, carried_in(): everything = jax.tree.map(lambda part: lax.all_gather(part, axis), value)  18.7 us
    unnamed x1, blocking collectives  17.1 us
    dot_general x1, matrix products, local(): jnp.dot(hidden, w_exp_down[0], preferred_element_type=jnp.float32)  10.1 us
    gather x1, local copies, waits for them, and re-layouts, local(): returned[slot_index].astype(jnp.float32)  7.96 us
  transfers between devices with their start and end apart: 4, of which 2 were waited for; matrix products, arithmetic and copies ran while one was open for 10% of the time, Pallas kernels for 0%

commit v1 on v0

v1 whole, which is shorter than its diff:
```python
import jax
import jax.numpy as jnp
import numpy as np
from jax import lax
from jax.sharding import Mesh, PartitionSpec as P

pool_windows = (2, 4, 8, 16, 16, 32, 64, 128)
alpha_mix = 8.0**0.25
norm_eps = 1e-05
SP = ("z", "x")
TP = ("y", "c")
PLANE = ("x", "y", "c")


def ring(value, axis, by):
    length = lax.axis_size(axis)
    return lax.ppermute(value, axis, [(i, (i + by) % length) for i in range(length)])


def shifted(value, axis, by):
    length = lax.axis_size(axis)
    pairs = [(i, i + by) for i in range(length) if 0 <= i + by < length]
    return lax.ppermute(value, axis, pairs)


def layer_norm(values, scales):
    center = values - jnp.mean(values, axis=-1, keepdims=True)
    spread = jnp.mean(center * center, axis=-1, keepdims=True)
    return center * lax.rsqrt(spread + norm_eps) * scales.astype(jnp.float32)


def swiglu_hidden(token_rows, gate_weight, up_weight):
    gate_vals = jnp.dot(token_rows, gate_weight, preferred_element_type=jnp.float32)
    up_vals = jnp.dot(token_rows, up_weight, preferred_element_type=jnp.float32)
    return (jax.nn.silu(gate_vals) * up_vals).astype(jnp.bfloat16)


def dot32(a, b):
    return jnp.dot(a, b, preferred_element_type=jnp.float32)


def gathered_rows(block):
    ny, nc = lax.axis_size("y"), lax.axis_size("c")
    y, c = lax.axis_index("y"), lax.axis_index("c")
    found = []
    part = block
    for i in range(ny):
        if i:
            part = ring(part, "y", 1)
        from_y = (y - i) % ny
        found.append((from_y * nc + c, part))
        other = part
        for j in range(1, nc):
            other = ring(other, "c", 1)
            found.append((from_y * nc + (c - j) % nc, other))
    return found


def pooled(pool_in, doc_ids, w_group, pool_scale):
    tok_count, local_width = pool_in.shape
    group_width = w_group.shape[1]
    group_count = local_width // group_width
    halo = max(pool_windows)
    tp_at = lax.axis_index(TP)
    sp_size, sp_at = lax.axis_size(SP), lax.axis_index(SP)
    before = shifted(pool_in[tok_count - halo :], SP, 1)
    last_doc = doc_ids[-1]
    trailing = (doc_ids == last_doc).astype(jnp.bfloat16)
    tail_sums = dot32(trailing[None, :], pool_in)
    tail_count = jnp.sum(trailing.astype(jnp.float32))
    lane = lax.broadcasted_iota(jnp.int32, (1, group_width), 1)
    info = jnp.where(lane == 0, last_doc.astype(jnp.float32), jnp.where(lane == 1, tail_count, 0.0))
    tail = jnp.concatenate([tail_sums, info], axis=1)
    tails = lax.all_to_all(
        jnp.broadcast_to(tail, (sp_size, tail.shape[1])), SP, split_axis=0, concat_axis=0, tiled=True
    )
    prev_doc = jnp.max(
        jnp.where(jnp.arange(sp_size) < sp_at, tails[:, local_width], -1.0)
    )
    joined = (jnp.arange(sp_size) < sp_at) & (tails[:, local_width] == prev_doc)
    prev = jnp.sum(jnp.where(joined[:, None], tails, 0.0), axis=0)
    prev_sums, prev_count = prev[:local_width], prev[local_width + 1]

    t = lax.broadcasted_iota(jnp.int32, (tok_count, tok_count), 0)
    s = lax.broadcasted_iota(jnp.int32, (tok_count, tok_count), 1)
    same = (doc_ids[:, None] == doc_ids[None, :]) & (s <= t)
    local_since = jnp.sum(same.astype(jnp.float32), axis=1) - 1.0
    running = dot32(same.astype(jnp.bfloat16), pool_in)
    table = jnp.asarray(pool_windows, dtype=jnp.int32)
    widths = [table[tp_at * group_count + g] for g in range(group_count)]
    recent = [
        dot32(
            (same & (s > t - widths[g])).astype(jnp.bfloat16),
            pool_in[:, g * group_width : (g + 1) * group_width],
        )
        for g in range(group_count)
    ]

    carried = doc_ids.astype(jnp.float32) == prev_doc
    since = (local_since + jnp.where(carried, prev_count, 0.0))[:, None]
    running = running + jnp.where(carried[:, None], prev_sums[None, :], 0.0)
    doc_mean = running / (since + 1.0)
    th = lax.broadcasted_iota(jnp.int32, (halo, halo), 0)
    sh = lax.broadcasted_iota(jnp.int32, (halo, halo), 1) - halo
    reach = (th - sh).astype(jnp.float32) <= since[:halo]
    local_groups = lax.dynamic_slice_in_dim(w_group, tp_at * group_count, group_count, 0)
    scale = lax.dynamic_slice_in_dim(pool_scale, tp_at * local_width, local_width, 0)
    scale = scale.astype(jnp.float32)[None, :]
    mixed = []
    for g in range(group_count):
        cols = slice(g * group_width, (g + 1) * group_width)
        early = dot32((reach & (sh > th - widths[g])).astype(jnp.bfloat16), before[:, cols])
        total = recent[g] + jnp.pad(early, ((0, tok_count - halo), (0, 0)))
        mean = total / jnp.minimum(since + 1.0, widths[g].astype(jnp.float32))
        offset = 0.5 * (mean + doc_mean[:, cols]) - pool_in[:, cols].astype(jnp.float32)
        rows = dot32(offset.astype(jnp.bfloat16), local_groups[g])
        mixed.append((rows * scale[:, cols]).astype(jnp.bfloat16))
    return jnp.concatenate(mixed, axis=1)


def slot_tables(packed, top, capacity):
    rows = packed.shape[1]
    per_plane = lax.axis_size(PLANE)
    first = lax.axis_index("z") * per_plane
    ids = packed[:top].astype(jnp.int32)
    experts = first + jnp.arange(per_plane, dtype=jnp.int32)
    hit = ids[:, None, :] == experts[None, :, None]
    member = jnp.any(hit, axis=0)
    weight = jnp.sum(jnp.where(hit, packed[top:][:, None, :], 0.0), axis=0)
    a = lax.broadcasted_iota(jnp.int32, (rows, rows), 0)
    b = lax.broadcasted_iota(jnp.int32, (rows, rows), 1)
    rank = dot32(member.astype(jnp.bfloat16), (a < b).astype(jnp.bfloat16)).astype(jnp.int32)
    slot = jnp.arange(capacity, dtype=jnp.int32)
    chosen = member[:, None, :] & (rank[:, None, :] == slot[None, :, None])
    slots = per_plane * capacity
    take = chosen.astype(jnp.bfloat16).reshape(slots, rows)
    spread = jnp.where(chosen, weight[:, None, :], 0.0).reshape(slots, rows)
    high = lax.reduce_precision(spread, 8, 7)
    give = jnp.concatenate([high, spread - high], axis=1).astype(jnp.bfloat16)
    return take, give


def local(
    resid,
    pool_in,
    doc_ids,
    w_group,
    pool_scale,
    w_branch,
    norm_gain,
    route_ids,
    route_wts,
    w_exp_gate,
    w_exp_up,
    w_exp_down,
    w_sh_gate,
    w_sh_up,
    w_sh_down,
    final_gain,
):
    row_count, model_width = resid.shape
    nz, per_plane, tp_size = lax.axis_size("z"), lax.axis_size(PLANE), lax.axis_size(TP)
    local_width = pool_in.shape[1]
    top = route_ids.shape[1]
    capacity = 2 * row_count * top // (nz * per_plane)
    packed = jnp.concatenate([route_ids.astype(jnp.float32), route_wts], axis=1).T
    tables = [
        slot_tables(ring(packed, "z", r) if r else packed, top, capacity) for r in range(nz)
    ]
    branch_rows = gathered_rows(w_branch)

    mixed = pooled(pool_in, doc_ids, w_group, pool_scale)
    parts = lax.all_to_all(
        mixed.reshape(tp_size, row_count, local_width), TP, split_axis=0, concat_axis=0, tiled=True
    )
    branch = 0.0
    for at, rows in branch_rows:
        branch = branch + dot32(lax.dynamic_index_in_dim(parts, at, 0, keepdims=False), rows)
    normed = layer_norm(alpha_mix * resid.astype(jnp.float32) + branch, norm_gain).astype(
        jnp.bfloat16
    )

    def across(value):
        value = value.reshape(per_plane, -1, model_width)
        value = lax.all_to_all(value, PLANE, split_axis=0, concat_axis=0, tiled=True)
        return value.reshape(-1, model_width)

    block = normed
    arrived = []
    for r in range(nz):
        if r:
            block = ring(block, "z", 1)
        arrived.append(across(dot32(tables[r][0], block).astype(jnp.bfloat16)))
    shared = dot32(swiglu_hidden(normed, w_sh_gate, w_sh_up), w_sh_down)

    routed = None
    for r in reversed(range(nz)):
        hidden = swiglu_hidden(arrived[r], w_exp_gate[0], w_exp_up[0])
        returned = across(dot32(hidden, w_exp_down[0]).astype(jnp.bfloat16))
        both = lax.dot_general(
            tables[r][1], returned, (((0,), (0,)), ((), ())), preferred_element_type=jnp.float32
        )
        partial = both[:row_count] + both[row_count:]
        routed = partial if routed is None else partial + routed.astype(jnp.float32)
        if r:
            routed = ring(routed.astype(jnp.bfloat16), "z", -1)
    return layer_norm(alpha_mix * normed.astype(jnp.float32) + routed + shared, final_gain).astype(
        jnp.bfloat16
    )


def axis_count(devices, at, whole):
    places = {getattr(d, "coords", (0, 0, 0))[at] for d in devices.flat}
    return len(places) if len(places) > 1 else whole


def solution(mesh):
    sp_size, tp_size = mesh.shape["sp"], mesh.shape["tp"]
    nz = axis_count(mesh.devices, 2, sp_size)
    ny = axis_count(mesh.devices, 1, tp_size)
    parted = Mesh(
        mesh.devices.reshape(nz, sp_size // nz, ny, tp_size // ny), ("z", "x", "y", "c")
    )
    every = SP + TP
    placed = (
        P(every, None),
        P(SP, TP),
        P(SP),
        P(),
        P(),
        P(TP, None),
        P(),
        P(every, None),
        P(every, None),
        P(every, None, None),
        P(every, None, None),
        P(every, None, None),
        P(),
        P(),
        P(),
        P(),
    )
    return jax.shard_map(
        local, mesh=parted, in_specs=placed, out_specs=P(every, None), check_vma=False
    )
```

time: 371 us -> 233 us (0.63)
  blocking collectives: 132 us -> 0 us
  starting transfers between devices: 12.3 us -> 55.6 us
  matrix products: 26.2 us -> 66.7 us
  local copies, waits for them, and re-layouts: 39.7 us -> 7.05 us
  waiting for transfers between devices: 97.8 us -> 69.7 us
  loops' own time: 23.8 us -> 0 us
  between operations: 14.4 us -> 2.65 us
  other arithmetic: 23.3 us -> 29.3 us
    all_to_all x1 -> x0, blocking collectives: 96.5 us -> none  [local(): lax.all_to_all(outgoing, ('sp', 'tp'), split_axis=0, concat_axis=0, tiled...]
    all_to_all x2 -> x10, waiting for transfers between devices: 97.8 us -> 43.7 us  [the longest x8 40.4 us: across(): lax.all_to_all(value, PLANE, split_axis=0, concat_axis=0, tiled=True)]
    all_to_all x2 -> x10, starting transfers between devices: 7.35 us -> 40.8 us  [the longest x8 34.1 us: across(): lax.all_to_all(value, PLANE, split_axis=0, concat_axis=0, tiled=True)]
    dot_general x5 -> x27, matrix products: 24.1 us -> 51.9 us  [the longest x23 44.9 us: dot32(): return jnp.dot(a, b, preferred_element_type=jnp.float32)]
    ppermute x0 -> x12, waiting for transfers between devices: none -> 26 us  [ring(): lax.ppermute(value, axis, [(i, (i + by) % length) for i in range(length)])]
    another operation x1 -> x0, loops' own time: 23.8 us -> none  [carried_in(): return lax.fori_loop(0, length, lap, start)]
    all_gather x1 -> x0, blocking collectives: 18.7 us -> none  [carried_in(): everything = jax.tree.map(lambda part: lax.all_gather(part, axis), value)]
    unnamed x1 -> x0, blocking collectives: 17.1 us -> none
  transfers between devices with their start and end apart: 4 -> 23, of which waited for: 2 -> 12; matrix products, arithmetic and copies ran while one was open for 10% -> 42% of each run, Pallas kernels for 0% -> 0%
where the time goes in v1:
time: 233 us; the launch traced here: 231 us
  waiting for transfers between devices  69.7 us (30%)
  matrix products  66.7 us (29%)
  starting transfers between devices  55.6 us (24%)
  other arithmetic  29.3 us (13%)
  local copies, waits for them, and re-layouts  7.05 us (3%)
  between operations  2.65 us (1%)
    dot_general x23, matrix products, dot32(): return jnp.dot(a, b, preferred_element_type=jnp.float32)  44.9 us
    all_to_all x8, waiting for transfers between devices, across(): lax.all_to_all(value, PLANE, split_axis=0, concat_axis=0, tiled=True)  40.4 us
    all_to_all x8, starting transfers between devices, across(): lax.all_to_all(value, PLANE, split_axis=0, concat_axis=0, tiled=True)  34.1 us
    ppermute x12, waiting for transfers between devices, ring(): lax.ppermute(value, axis, [(i, (i + by) % length) for i in range(length)])  26 us
    dot_general x5, matrix products, swiglu_hidden(): jnp.dot(token_rows, gate_weight, preferred_element_type=jnp.float32)  14.8 us
    ppermute x12, starting transfers between devices, ring(): lax.ppermute(value, axis, [(i, (i + by) % length) for i in range(length)])  11 us
    dot_general x4, matrix products, local(): lax.dot_general(tables[r][1], returned, (((0,), (0,)), ((), ())), preferr...  7.05 us
    convert_element_type x3, other arithmetic, local(): routed = ring(routed.astype(jnp.bfloat16), 'z', -1)  4.98 us
  transfers between devices with their start and end apart: 23, of which 12 were waited for; matrix products, arithmetic and copies ran while one was open for 42% of the time, Pallas kernels for 0%

profile of v1, /device:TPU:0, one launch (start us, length us, event | category | flops | bytes accessed | tf_op | source)
XLA Modules:
  0.0 231.0 jit_solution(8430558439614243523)
XLA Ops:
  0.5 2.6 %collective-permute-start.2 = (bf16[256,2048]{1,0:T(8,128)(2,1)}, bf16[256,2048]{1,0:T(8,128)(2,1)}, u32[]{:S(2)}, u32[]{:S(2)}) collective-permute-start(bf16[256,2048]{1,0:T(8,128)(2,1)} %param.22), channel_id=1, source_target_pairs={{0,2},{2,0},{1,3},{3,1},{4,6},{6,4},{5,7},{7,5},{8,10},{10,8},{9,1... | collective-permute-start | bytes 3145736 | tf_op jit(solution)/shard_map/ppermute | solution.py:17
  4.4 1.6 collective-permute-start.4
  6.0 2.6 %collective-permute-start.6 = (f32[8,128]{1,0:T(8,128)S(1)}, f32[8,128]{1,0:T(8,128)S(1)}, u32[]{:S(2)}, u32[]{:S(2)}) collective-permute-start(f32[8,128]{1,0:T(8,128)S(1)} %maximum_bitcast_fusion), channel_id=1, source_target_pairs={{0,16},{8,24},{16,0},{24,8},{1,17},{9,25},{17,1},{25,9},{2,18},{10... | collective-permute-start | bytes 12296 | tf_op jit(solution)/shard_map/ppermute | solution.py:17
  8.6 1.3 collective-permute-start.8
  10.0 1.3 slice.101
  11.2 2.0 convert_reduce_fusion.1
  14.6 1.1 fusion.211
  16.3 3.3 %all-to-all-start = ((f32[8,1,384]{2,1,0:T(1,128)}), f32[8,1,384]{2,1,0:T(1,128)S(1)}, u32[]{:S(2)}, u32[]{:S(2)}) async-start(f32[8,1,384]{2,1,0:T(1,128)} %broadcast_in_dim.181), calls=%async_computation | async-start | bytes 24576 | tf_op jit(solution)/shard_map/all_to_all | solution.py:74
  20.7 1.4 fusion.209
  24.1 1.1 iota_subtract_fusion
  30.4 3.8 %collective-permute-start = (bf16[128,256]{1,0:T(8,128)(2,1)S(1)}, bf16[128,256]{1,0:T(8,128)(2,1)S(1)}, u32[]{:S(2)}, u32[]{:S(2)}) collective-permute-start(bf16[128,256]{1,0:T(8,128)(2,1)S(1)} %slice.105), channel_id=1, source_target_pairs={{0,4},{4,8},{8,12},{12,16},{16,20},{20,24},{24,28},{1,5},{5,9},{9,... | collective-permute-start | bytes 196616 | tf_op jit(solution)/shard_map/ppermute | solution.py:23
  40.5 2.0 broadcast_minimum_fusion.1
  43.1 1.3 fusion.33
  44.8 1.3 fusion.46
  46.9 2.2 fusion.47
  51.0 3.4 %all-to-all-start.1 = ((bf16[4,128,256]{2,1,0:T(8,128)(2,1)}), bf16[4,128,256]{2,1,0:T(8,128)(2,1)S(1)}, u32[]{:S(2)}, u32[]{:S(2)}) async-start(bf16[4,128,256]{2,1,0:T(8,128)(2,1)} %bitcast.229), calls=%async_computation.1 | async-start | bytes 524288 | tf_op jit(solution)/shard_map/all_to_all | solution.py:173
  55.7 1.5 fusion.134
  57.1 3.2 %all-to-all-done.1 = bf16[4,128,256]{2,1,0:T(8,128)(2,1)S(1)} async-done(((bf16[4,128,256]{2,1,0:T(8,128)(2,1)}), bf16[4,128,256]{2,1,0:T(8,128)(2,1)S(1)}, u32[]{:S(2)}, u32[]{:S(2)}) %all-to-all-start.1) | async-done | bytes 262176 | tf_op jit(solution)/shard_map/all_to_all | solution.py:173
  60.7 1.5 convolution_add_fusion.2
  62.2 1.6 convolution_add_fusion.1
  63.9 1.6 fusion.210
  66.8 1.5 collective-permute-start.5
  68.3 2.5 %convolution_convert_fusion.7 = bf16[256,2048]{1,0:T(8,128)(2,1)} fusion(pred[256,128]{1,0:T(32,128)(4,1)S(1)} %get-tuple-element.44, bf16[128,2048]{1,0:T(8,128)(2,1)} %multiply_convert_fusion.1), kind=kOutput, calls=%fused_computation.7 | convolution fusion | flops 134742016 | bytes 1605632 | tf_op jit(solution)/shard_map/dot_general | solution.py:39
  70.7 4.2 %all-to-all-start.2 = ((bf16[8,32,2048]{2,1,0:T(8,128)(2,1)}), bf16[8,32,2048]{2,1,0:T(8,128)(2,1)}, u32[]{:S(2)}, u32[]{:S(2)}) async-start(bf16[8,32,2048]{2,1,0:T(8,128)(2,1)} %bitcast.224), calls=%async_computation.2 | async-start | bytes 2097152 | tf_op jit(solution)/shard_map/all_to_all | solution.py:185
  75.0 7.3 %collective-permute-done.5 = bf16[128,2048]{1,0:T(8,128)(2,1)} collective-permute-done((bf16[128,2048]{1,0:T(8,128)(2,1)}, bf16[128,2048]{1,0:T(8,128)(2,1)}, u32[]{:S(2)}, u32[]{:S(2)}) %collective-permute-start.5) | collective-permute-done | bytes 524320 | tf_op jit(solution)/shard_map/ppermute | solution.py:17
  82.3 2.5 %convolution_convert_fusion.5 = bf16[256,2048]{1,0:T(8,128)(2,1)} fusion(pred[256,128]{1,0:T(32,128)(4,1)S(1)} %get-tuple-element.45, bf16[128,2048]{1,0:T(8,128)(2,1)} %collective-permute-done.5), kind=kOutput, calls=%fused_computation.5 | convolution fusion | flops 134742016 | bytes 1605632 | tf_op jit(solution)/shard_map/dot_general | solution.py:39
  84.8 4.7 %all-to-all-done.2 = bf16[8,32,2048]{2,1,0:T(8,128)(2,1)} async-done(((bf16[8,32,2048]{2,1,0:T(8,128)(2,1)}), bf16[8,32,2048]{2,1,0:T(8,128)(2,1)}, u32[]{:S(2)}, u32[]{:S(2)}) %all-to-all-start.2) | async-done | bytes 1048608 | tf_op jit(solution)/shard_map/all_to_all | solution.py:185
  89.5 4.2 %all-to-all-start.4 = ((bf16[8,32,2048]{2,1,0:T(8,128)(2,1)}), bf16[8,32,2048]{2,1,0:T(8,128)(2,1)}, u32[]{:S(2)}, u32[]{:S(2)}) async-start(bf16[8,32,2048]{2,1,0:T(8,128)(2,1)} %bitcast.222), calls=%async_computation.4 | async-start | bytes 2097152 | tf_op jit(solution)/shard_map/all_to_all | solution.py:185
  93.9 3.0 %collective-permute-done.7 = bf16[128,2048]{1,0:T(8,128)(2,1)} collective-permute-done((bf16[128,2048]{1,0:T(8,128)(2,1)}, bf16[128,2048]{1,0:T(8,128)(2,1)}, u32[]{:S(2)}, u32[]{:S(2)}) %collective-permute-start.7) | collective-permute-done | bytes 524320 | tf_op jit(solution)/shard_map/ppermute | solution.py:17
  96.9 13.7 %collective-permute-done.9 = bf16[128,2048]{1,0:T(8,128)(2,1)S(1)} collective-permute-done((bf16[128,2048]{1,0:T(8,128)(2,1)}, bf16[128,2048]{1,0:T(8,128)(2,1)S(1)}, u32[]{:S(2)}, u32[]{:S(2)}) %collective-permute-start.9) | collective-permute-done | bytes 524320 | tf_op jit(solution)/shard_map/ppermute | solution.py:17
  110.6 1.4 convolution_convert_fusion.1
  112.0 4.2 %all-to-all-start.8 = ((bf16[8,32,2048]{2,1,0:T(8,128)(2,1)}), bf16[8,32,2048]{2,1,0:T(8,128)(2,1)}, u32[]{:S(2)}, u32[]{:S(2)}) async-start(bf16[8,32,2048]{2,1,0:T(8,128)(2,1)} %bitcast.221), calls=%async_computation.8 | async-start | bytes 2097152 | tf_op jit(solution)/shard_map/all_to_all | solution.py:185
  116.5 1.0 reduce-precision_convert_fusion.3
  117.5 2.2 fusion.212
  119.8 2.5 %convolution_convert_fusion.3 = bf16[256,2048]{1,0:T(8,128)(2,1)} fusion(pred[256,128]{1,0:T(32,128)(4,1)S(1)} %copy-done.5, bf16[128,2048]{1,0:T(8,128)(2,1)} %collective-permute-done.7), kind=kOutput, calls=%fused_computation.3 | convolution fusion | flops 134742016 | bytes 1605632 | tf_op jit(solution)/shard_map/dot_general | solution.py:39
  122.3 8.4 %all-to-all-done.8 = bf16[8,32,2048]{2,1,0:T(8,128)(2,1)} async-done(((bf16[8,32,2048]{2,1,0:T(8,128)(2,1)}), bf16[8,32,2048]{2,1,0:T(8,128)(2,1)}, u32[]{:S(2)}, u32[]{:S(2)}) %all-to-all-start.8) | async-done | bytes 1048608 | tf_op jit(solution)/shard_map/all_to_all | solution.py:185
  130.7 4.3 %all-to-all-start.6 = ((bf16[8,32,2048]{2,1,0:T(8,128)(2,1)}), bf16[8,32,2048]{2,1,0:T(8,128)(2,1)}, u32[]{:S(2)}, u32[]{:S(2)}) async-start(bf16[8,32,2048]{2,1,0:T(8,128)(2,1)} %bitcast.223), calls=%async_computation.6 | async-start | bytes 2097152 | tf_op jit(solution)/shard_map/all_to_all | solution.py:185
  135.0 3.6 %fusion.19 = f32[256,512]{1,0:T(8,128)} fusion(bf16[256,2048]{1,0:T(8,128)(2,1)} %bitcast.20, bf16[1,2048,512]{2,1,0:T(8,128)(2,1)} %param.26), kind=kOutput, calls=%fused_computation.30 | convolution fusion | flops 536870912 | bytes 3670016 | tf_op jit(solution)/shard_map/dot_general | solution.py:33
  138.5 2.7 %fusion.13 = f32[256,512]{1,0:T(8,128)} fusion(bf16[256,2048]{1,0:T(8,128)(2,1)} %bitcast.44, bf16[1,2048,512]{2,1,0:T(8,128)(2,1)S(1)} %copy-done.40), kind=kOutput, calls=%fused_computation.24 | convolution fusion | flops 536870912 | bytes 3670016 | tf_op jit(solution)/shard_map/dot_general | solution.py:33
  141.2 4.3 %convolution_convert_fusion = bf16[256,2048]{1,0:T(8,128)(2,1)} fusion(bf16[1,512,2048]{2,1,0:T(8,128)(2,1)S(1)} %copy-done, bf16[256,2048]{1,0:T(8,128)(2,1)} %bitcast.44, bf16[1,2048,512]{2,1,0:T(8,128)(2,1)} %param.27, f32[256,512]{1,0:T(8,128)} %fusion.13), kind=kOutput, calls=%fused_computation | convolution fusion | flops 1075052544 | bytes 6815744 | tf_op jit(solution)/shard_map/dot_general | solution.py:39
  145.6 3.9 %all-to-all-done.6 = bf16[8,32,2048]{2,1,0:T(8,128)(2,1)} async-done(((bf16[8,32,2048]{2,1,0:T(8,128)(2,1)}), bf16[8,32,2048]{2,1,0:T(8,128)(2,1)}, u32[]{:S(2)}, u32[]{:S(2)}) %all-to-all-start.6) | async-done | bytes 1048608 | tf_op jit(solution)/shard_map/all_to_all | solution.py:185
  149.4 4.4 %all-to-all-start.9 = ((bf16[8,32,2048]{2,1,0:T(8,128)(2,1)}), bf16[8,32,2048]{2,1,0:T(8,128)(2,1)}, u32[]{:S(2)}, u32[]{:S(2)}) async-start(bf16[8,32,2048]{2,1,0:T(8,128)(2,1)} %bitcast.228), calls=%async_computation.9 | async-start | bytes 2097152 | tf_op jit(solution)/shard_map/all_to_all | solution.py:185
  153.9 3.5 %fusion.17 = f32[256,512]{1,0:T(8,128)} fusion(bf16[256,2048]{1,0:T(8,128)(2,1)} %bitcast.30, bf16[1,2048,512]{2,1,0:T(8,128)(2,1)} %param.26), kind=kOutput, calls=%fused_computation.28 | convolution fusion | flops 536870912 | bytes 3670016 | tf_op jit(solution)/shard_map/dot_general | solution.py:33
  157.4 2.8 %fusion.15 = f32[256,512]{1,0:T(8,128)} fusion(bf16[256,2048]{1,0:T(8,128)(2,1)} %bitcast.37, bf16[1,2048,512]{2,1,0:T(8,128)(2,1)S(1)} %copy-done.41), kind=kOutput, calls=%fused_computation.26 | convolution fusion | flops 536870912 | bytes 3670016 | tf_op jit(solution)/shard_map/dot_general | solution.py:33
  160.2 4.4 %convolution_convert_fusion.2 = bf16[256,2048]{1,0:T(8,128)(2,1)} fusion(bf16[1,512,2048]{2,1,0:T(8,128)(2,1)S(1)} %copy-done, bf16[256,2048]{1,0:T(8,128)(2,1)} %bitcast.37, bf16[1,2048,512]{2,1,0:T(8,128)(2,1)} %param.27, f32[256,512]{1,0:T(8,128)} %fusion.15), kind=kOutput, calls=%fused_computation.2 | convolution fusion | flops 1075052544 | bytes 6815744 | tf_op jit(solution)/shard_map/dot_general | solution.py:39
  164.5 3.6 %all-to-all-done.9 = bf16[8,32,2048]{2,1,0:T(8,128)(2,1)} async-done(((bf16[8,32,2048]{2,1,0:T(8,128)(2,1)}), bf16[8,32,2048]{2,1,0:T(8,128)(2,1)}, u32[]{:S(2)}, u32[]{:S(2)}) %all-to-all-start.9) | async-done | bytes 1048608 | tf_op jit(solution)/shard_map/all_to_all | solution.py:185
  168.1 4.3 %all-to-all-start.7 = ((bf16[8,32,2048]{2,1,0:T(8,128)(2,1)}), bf16[8,32,2048]{2,1,0:T(8,128)(2,1)}, u32[]{:S(2)}, u32[]{:S(2)}) async-start(bf16[8,32,2048]{2,1,0:T(8,128)(2,1)} %bitcast.227), calls=%async_computation.7 | async-start | bytes 2097152 | tf_op jit(solution)/shard_map/all_to_all | solution.py:185
  172.4 1.8 fusion.129
  175.2 4.3 %convolution_convert_fusion.4 = bf16[256,2048]{1,0:T(8,128)(2,1)} fusion(bf16[1,512,2048]{2,1,0:T(8,128)(2,1)S(1)} %copy-done, bf16[256,2048]{1,0:T(8,128)(2,1)} %bitcast.30, bf16[1,2048,512]{2,1,0:T(8,128)(2,1)} %param.27, f32[256,512]{1,0:T(8,128)} %fusion.17), kind=kOutput, calls=%fused_computation.4 | convolution fusion | flops 1075052544 | bytes 6815744 | tf_op jit(solution)/shard_map/dot_general | solution.py:39
  179.6 7.3 %all-to-all-done.7 = bf16[8,32,2048]{2,1,0:T(8,128)(2,1)} async-done(((bf16[8,32,2048]{2,1,0:T(8,128)(2,1)}), bf16[8,32,2048]{2,1,0:T(8,128)(2,1)}, u32[]{:S(2)}, u32[]{:S(2)}) %all-to-all-start.7) | async-done | bytes 1048608 | tf_op jit(solution)/shard_map/all_to_all | solution.py:185
  186.9 4.2 %all-to-all-start.5 = ((bf16[8,32,2048]{2,1,0:T(8,128)(2,1)}), bf16[8,32,2048]{2,1,0:T(8,128)(2,1)}, u32[]{:S(2)}, u32[]{:S(2)}) async-start(bf16[8,32,2048]{2,1,0:T(8,128)(2,1)} %bitcast.225), calls=%async_computation.5 | async-start | bytes 2097152 | tf_op jit(solution)/shard_map/all_to_all | solution.py:185
  191.1 1.8 fusion.125
  192.9 2.0 fusion.52
  195.1 4.3 %convolution_convert_fusion.6 = bf16[256,2048]{1,0:T(8,128)(2,1)} fusion(bf16[1,512,2048]{2,1,0:T(8,128)(2,1)S(1)} %copy-done, bf16[256,2048]{1,0:T(8,128)(2,1)} %bitcast.20, bf16[1,2048,512]{2,1,0:T(8,128)(2,1)} %param.27, f32[256,512]{1,0:T(8,128)} %fusion.19), kind=kOutput, calls=%fused_computation.6 | convolution fusion | flops 1075052544 | bytes 6815744 | tf_op jit(solution)/shard_map/dot_general | solution.py:39
  199.4 6.2 %all-to-all-done.5 = bf16[8,32,2048]{2,1,0:T(8,128)(2,1)} async-done(((bf16[8,32,2048]{2,1,0:T(8,128)(2,1)}), bf16[8,32,2048]{2,1,0:T(8,128)(2,1)}, u32[]{:S(2)}, u32[]{:S(2)}) %all-to-all-start.5) | async-done | bytes 1048608 | tf_op jit(solution)/shard_map/all_to_all | solution.py:185
  205.6 4.2 %all-to-all-start.3 = ((bf16[8,32,2048]{2,1,0:T(8,128)(2,1)}), bf16[8,32,2048]{2,1,0:T(8,128)(2,1)}, u32[]{:S(2)}, u32[]{:S(2)}) async-start(bf16[8,32,2048]{2,1,0:T(8,128)(2,1)} %bitcast.226), calls=%async_computation.3 | async-start | bytes 2097152 | tf_op jit(solution)/shard_map/all_to_all | solution.py:185
  209.8 1.8 fusion.121
  211.6 2.0 fusion.54
  213.8 4.2 %fusion.49 = f32[128,2048]{1,0:T(8,128)} fusion(bf16[512,2048]{1,0:T(8,128)(2,1)} %param.31, bf16[128,2048]{1,0:T(8,128)(2,1)} %multiply_convert_fusion.1, bf16[2048,512]{1,0:T(8,128)(2,1)} %param.30, f32[128,512]{1,0:T(8,128)S(1)} %fusion.212), kind=kOutput, calls=%fused_computation.48 | convolution fusion | flops 537264128 | bytes 6029312 | tf_op jit(solution)/shard_map/dot_general | solution.py:39
  218.0 6.3 %all-to-all-done.3 = bf16[8,32,2048]{2,1,0:T(8,128)(2,1)} async-done(((bf16[8,32,2048]{2,1,0:T(8,128)(2,1)}), bf16[8,32,2048]{2,1,0:T(8,128)(2,1)}, u32[]{:S(2)}, u32[]{:S(2)}) %all-to-all-start.3) | async-done | bytes 1048608 | tf_op jit(solution)/shard_map/all_to_all | solution.py:185
  224.3 1.8 fusion.117
  226.1 2.1 collective-permute-done.12
  228.2 1.5 fusion.203
  230.0 1.0 multiply_convert_fusion
  (154 shorter events, 24.6 us)
Async XLA Ops:
  0.0 141.2 %copy-start = (bf16[1,512,2048]{2,1,0:T(8,128)(2,1)S(1)}, bf16[1,512,2048]{2,1,0:T(8,128)(2,1)}, u32[]{:S(2)}) copy-start(bf16[1,512,2048]{2,1,0:T(8,128)(2,1)} %param.28) | copy-start | bytes 6291460
  0.0 60.7 %collective-permute-start.1 = (bf16[256,2048]{1,0:T(8,128)(2,1)}, bf16[256,2048]{1,0:T(8,128)(2,1)}, u32[]{:S(2)}, u32[]{:S(2)}) collective-permute-start(bf16[256,2048]{1,0:T(8,128)(2,1)} %param.22), channel_id=1, source_target_pairs={{0,1},{1,0},{2,3},{3,2},{4,5},{5,4},{6,7},{7,6},{8,9},{9,8},{10,11... | collective-permute-start | bytes 3145736 | tf_op jit(solution)/shard_map/ppermute | solution.py:17
  0.5 53.9 %collective-permute-start.2 = (bf16[256,2048]{1,0:T(8,128)(2,1)}, bf16[256,2048]{1,0:T(8,128)(2,1)}, u32[]{:S(2)}, u32[]{:S(2)}) collective-permute-start(bf16[256,2048]{1,0:T(8,128)(2,1)} %param.22), channel_id=1, source_target_pairs={{0,2},{2,0},{1,3},{3,1},{4,6},{6,4},{5,7},{7,5},{8,10},{10,8},{9,1... | collective-permute-start | bytes 3145736 | tf_op jit(solution)/shard_map/ppermute | solution.py:17
  4.4 26.0 %collective-permute-start.4 = (f32[8,128]{1,0:T(8,128)S(1)}, f32[8,128]{1,0:T(8,128)S(1)}, u32[]{:S(2)}, u32[]{:S(2)}) collective-permute-start(f32[8,128]{1,0:T(8,128)S(1)} %maximum_bitcast_fusion), channel_id=1, source_target_pairs={{0,8},{8,16},{16,24},{24,0},{1,9},{9,17},{17,25},{25,1},{2,10},{10... | collective-permute-start | bytes 12296 | tf_op jit(solution)/shard_map/ppermute | solution.py:17
  6.0 28.8 %collective-permute-start.6 = (f32[8,128]{1,0:T(8,128)S(1)}, f32[8,128]{1,0:T(8,128)S(1)}, u32[]{:S(2)}, u32[]{:S(2)}) collective-permute-start(f32[8,128]{1,0:T(8,128)S(1)} %maximum_bitcast_fusion), channel_id=1, source_target_pairs={{0,16},{8,24},{16,0},{24,8},{1,17},{9,25},{17,1},{25,9},{2,18},{10... | collective-permute-start | bytes 12296 | tf_op jit(solution)/shard_map/ppermute | solution.py:17
  8.6 26.8 %collective-permute-start.8 = (f32[8,128]{1,0:T(8,128)S(1)}, f32[8,128]{1,0:T(8,128)S(1)}, u32[]{:S(2)}, u32[]{:S(2)}) collective-permute-start(f32[8,128]{1,0:T(8,128)S(1)} %maximum_bitcast_fusion), channel_id=1, source_target_pairs={{0,24},{8,0},{16,8},{24,16},{1,25},{9,1},{17,9},{25,17},{2,26},{10... | collective-permute-start | bytes 12296 | tf_op jit(solution)/shard_map/ppermute | solution.py:17
  15.7 29.0 %copy-start.4 = (bf16[512,256]{1,0:T(8,128)(2,1)S(1)}, bf16[512,256]{1,0:T(8,128)(2,1)}, u32[]{:S(2)}) copy-start(bf16[512,256]{1,0:T(8,128)(2,1)} %param.18) | copy-start | bytes 786436
  15.7 29.1 %copy-start.6 = (s32[512]{0:T(512)S(1)}, s32[512]{0:T(512)}, u32[]{:S(2)}) copy-start(s32[512]{0:T(512)} %param.19) | copy-start | bytes 6148
  16.3 22.0 %all-to-all-start = ((f32[8,1,384]{2,1,0:T(1,128)}), f32[8,1,384]{2,1,0:T(1,128)S(1)}, u32[]{:S(2)}, u32[]{:S(2)}) async-start(f32[8,1,384]{2,1,0:T(1,128)} %broadcast_in_dim.181), calls=%async_computation | async-start | bytes 24576 | tf_op jit(solution)/shard_map/all_to_all | solution.py:74
  25.8 12.5 %copy-start.7 = (s32[4,128]{1,0:T(4,128)}, s32[4,128]{1,0:T(4,128)S(1)}, u32[]{:S(2)}) copy-start(s32[4,128]{1,0:T(4,128)S(1)} %get-tuple-element.29) | copy-start | bytes 6148
  27.1 17.6 %copy-start.38 = (s32[8]{0:T(128)}, s32[8]{0:T(128)S(1)}, u32[]{:S(2)}) copy-start(s32[8]{0:T(128)S(1)} %iota_add_fusion) | copy-start | bytes 100
  30.4 14.0 %collective-permute-start = (bf16[128,256]{1,0:T(8,128)(2,1)S(1)}, bf16[128,256]{1,0:T(8,128)(2,1)S(1)}, u32[]{:S(2)}, u32[]{:S(2)}) collective-permute-start(bf16[128,256]{1,0:T(8,128)(2,1)S(1)} %slice.105), channel_id=1, source_target_pairs={{0,4},{4,8},{8,12},{12,16},{16,20},{20,24},{24,28},{1,5},{5,9},{9,... | collective-permute-start | bytes 196616 | tf_op jit(solution)/shard_map/ppermute | solution.py:23
  34.8 3.4 %copy-start.9 = (s32[4,128]{1,0:T(4,128)}, s32[4,128]{1,0:T(4,128)S(1)}, u32[]{:S(2)}) copy-start(s32[4,128]{1,0:T(4,128)S(1)} %get-tuple-element.31) | copy-start | bytes 6148
  35.4 2.8 %copy-start.11 = (s32[4,128]{1,0:T(4,128)}, s32[4,128]{1,0:T(4,128)S(1)}, u32[]{:S(2)}) copy-start(s32[4,128]{1,0:T(4,128)S(1)} %get-tuple-element.33) | copy-start | bytes 6148
  36.0 8.7 %copy-start.13 = (s32[4,128]{1,0:T(4,128)}, s32[4,128]{1,0:T(4,128)S(1)}, u32[]{:S(2)}) copy-start(s32[4,128]{1,0:T(4,128)S(1)} %get-tuple-element.35) | copy-start | bytes 6148
  36.7 8.0 %copy-start.22 = (pred[8,128]{1,0:T(8,128)(4,1)}, pred[8,128]{1,0:T(8,128)(4,1)S(1)}, u32[]{:S(2)}) copy-start(pred[8,128]{1,0:T(8,128)(4,1)S(1)} %get-tuple-element.9) | copy-start | bytes 3076
  36.7 8.0 %copy-start.24 = (pred[8,128]{1,0:T(8,128)(4,1)}, pred[8,128]{1,0:T(8,128)(4,1)S(1)}, u32[]{:S(2)}) copy-start(pred[8,128]{1,0:T(8,128)(4,1)S(1)} %get-tuple-element.10) | copy-start | bytes 3076
  36.7 8.1 %copy-start.27 = (pred[8,128]{1,0:T(8,128)(4,1)}, pred[8,128]{1,0:T(8,128)(4,1)S(1)}, u32[]{:S(2)}) copy-start(pred[8,128]{1,0:T(8,128)(4,1)S(1)} %get-tuple-element.12) | copy-start | bytes 3076
  36.8 18.8 %copy-start.15 = (s32[8,128]{1,0:T(8,128)}, s32[8,128]{1,0:T(8,128)S(1)}, u32[]{:S(2)}) copy-start(s32[8,128]{1,0:T(8,128)S(1)} %convolution_convert_fusion.10) | copy-start | bytes 12292
  46.9 13.4 %copy-start.2 = (bf16[256,2048]{1,0:T(8,128)(2,1)S(1)}, bf16[256,2048]{1,0:T(8,128)(2,1)}, u32[]{:S(2)}) copy-start(bf16[256,2048]{1,0:T(8,128)(2,1)} %param.22) | copy-start | bytes 3145732
  51.0 9.4 %all-to-all-start.1 = ((bf16[4,128,256]{2,1,0:T(8,128)(2,1)}), bf16[4,128,256]{2,1,0:T(8,128)(2,1)S(1)}, u32[]{:S(2)}, u32[]{:S(2)}) async-start(bf16[4,128,256]{2,1,0:T(8,128)(2,1)} %bitcast.229), calls=%async_computation.1 | async-start | bytes 524288 | tf_op jit(solution)/shard_map/all_to_all | solution.py:173
  54.4 9.5 %collective-permute-start.3 = (bf16[256,2048]{1,0:T(8,128)(2,1)}, bf16[256,2048]{1,0:T(8,128)(2,1)}, u32[]{:S(2)}, u32[]{:S(2)}) collective-permute-start(bf16[256,2048]{1,0:T(8,128)(2,1)} %collective-permute-done.2), channel_id=1, source_target_pairs={{0,1},{1,0},{2,3},{3,2},{4,5},{5,4},{6,7},{7,6},{8,9},{9,8},{10,11... | collective-permute-start | bytes 3145736 | tf_op jit(solution)/shard_map/ppermute | solution.py:17
  55.7 6.6 %copy-start.19 = (s32[8,128]{1,0:T(8,128)}, s32[8,128]{1,0:T(8,128)S(1)}, u32[]{:S(2)}) copy-start(s32[8,128]{1,0:T(8,128)S(1)} %convolution_convert_fusion.9) | copy-start | bytes 12292
  65.5 5.2 %copy-start.33 = (f32[128]{0:T(128)}, f32[128]{0:T(128)S(1)}, u32[]{:S(2)}) copy-start(f32[128]{0:T(128)S(1)} %broadcast_multiply_fusion.1) | copy-start | bytes 1540
  65.8 5.0 %copy-start.36 = (f32[128]{0:T(128)}, f32[128]{0:T(128)S(1)}, u32[]{:S(2)}) copy-start(f32[128]{0:T(128)S(1)} %add_rsqrt_fusion.1) | copy-start | bytes 1540
  66.8 15.5 %collective-permute-start.5 = (bf16[128,2048]{1,0:T(8,128)(2,1)}, bf16[128,2048]{1,0:T(8,128)(2,1)}, u32[]{:S(2)}, u32[]{:S(2)}) collective-permute-start(bf16[128,2048]{1,0:T(8,128)(2,1)} %multiply_convert_fusion.1), channel_id=1, source_target_pairs={{0,8},{8,16},{16,24},{24,0},{1,9},{9,17},{17,25},{25,1},{2,10},{10... | collective-permute-start | bytes 1572872 | tf_op jit(solution)/shard_map/ppermute | solution.py:17
  70.7 18.7 %all-to-all-start.2 = ((bf16[8,32,2048]{2,1,0:T(8,128)(2,1)}), bf16[8,32,2048]{2,1,0:T(8,128)(2,1)}, u32[]{:S(2)}, u32[]{:S(2)}) async-start(bf16[8,32,2048]{2,1,0:T(8,128)(2,1)} %bitcast.224), calls=%async_computation.2 | async-start | bytes 2097152 | tf_op jit(solution)/shard_map/all_to_all | solution.py:185
  82.3 14.6 %collective-permute-start.7 = (bf16[128,2048]{1,0:T(8,128)(2,1)}, bf16[128,2048]{1,0:T(8,128)(2,1)}, u32[]{:S(2)}, u32[]{:S(2)}) collective-permute-start(bf16[128,2048]{1,0:T(8,128)(2,1)} %collective-permute-done.5), channel_id=1, source_target_pairs={{0,8},{8,16},{16,24},{24,0},{1,9},{9,17},{17,25},{25,1},{2,10},{10... | collective-permute-start | bytes 1572872 | tf_op jit(solution)/shard_map/ppermute | solution.py:17
  89.5 22.5 %all-to-all-start.4 = ((bf16[8,32,2048]{2,1,0:T(8,128)(2,1)}), bf16[8,32,2048]{2,1,0:T(8,128)(2,1)}, u32[]{:S(2)}, u32[]{:S(2)}) async-start(bf16[8,32,2048]{2,1,0:T(8,128)(2,1)} %bitcast.222), calls=%async_computation.4 | async-start | bytes 2097152 | tf_op jit(solution)/shard_map/all_to_all | solution.py:185
  93.7 22.5 %copy-start.35 = (bf16[2048]{0:T(1024)(128)(2,1)S(1)}, bf16[2048]{0:T(1024)(128)(2,1)}, u32[]{:S(2)}) copy-start(bf16[2048]{0:T(1024)(128)(2,1)} %param.32) | copy-start | bytes 12292
  93.7 22.5 %copy-start.8 = (s32[4,128]{1,0:T(4,128)S(1)}, s32[4,128]{1,0:T(4,128)}, u32[]{:S(2)}) copy-start(s32[4,128]{1,0:T(4,128)} %copy-done.7) | copy-start | bytes 6148
  93.7 22.5 %copy-start.10 = (s32[4,128]{1,0:T(4,128)S(1)}, s32[4,128]{1,0:T(4,128)}, u32[]{:S(2)}) copy-start(s32[4,128]{1,0:T(4,128)} %copy-done.9) | copy-start | bytes 6148
  93.7 22.5 %copy-start.12 = (s32[4,128]{1,0:T(4,128)S(1)}, s32[4,128]{1,0:T(4,128)}, u32[]{:S(2)}) copy-start(s32[4,128]{1,0:T(4,128)} %copy-done.11) | copy-start | bytes 6148
  93.7 22.5 %copy-start.14 = (s32[4,128]{1,0:T(4,128)S(1)}, s32[4,128]{1,0:T(4,128)}, u32[]{:S(2)}) copy-start(s32[4,128]{1,0:T(4,128)} %copy-done.13) | copy-start | bytes 6148
  93.8 22.5 %copy-start.29 = (f32[4,128]{1,0:T(4,128)S(1)}, f32[4,128]{1,0:T(4,128)}, u32[]{:S(2)}) copy-start(f32[4,128]{1,0:T(4,128)} %get-tuple-element.28) | copy-start | bytes 6148
  93.8 22.5 %copy-start.30 = (f32[4,128]{1,0:T(4,128)S(1)}, f32[4,128]{1,0:T(4,128)}, u32[]{:S(2)}) copy-start(f32[4,128]{1,0:T(4,128)} %get-tuple-element.30) | copy-start | bytes 6148
  93.8 22.5 %copy-start.31 = (f32[4,128]{1,0:T(4,128)S(1)}, f32[4,128]{1,0:T(4,128)}, u32[]{:S(2)}) copy-start(f32[4,128]{1,0:T(4,128)} %get-tuple-element.32) | copy-start | bytes 6148
  93.8 22.5 %copy-start.32 = (f32[4,128]{1,0:T(4,128)S(1)}, f32[4,128]{1,0:T(4,128)}, u32[]{:S(2)}) copy-start(f32[4,128]{1,0:T(4,128)} %get-tuple-element.34) | copy-start | bytes 6148
  93.8 22.5 %copy-start.39 = (s32[8]{0:T(128)S(1)}, s32[8]{0:T(128)}, u32[]{:S(2)}) copy-start(s32[8]{0:T(128)} %copy-done.38) | copy-start | bytes 100
  93.8 22.6 %copy-start.16 = (s32[8,128]{1,0:T(8,128)S(1)}, s32[8,128]{1,0:T(8,128)}, u32[]{:S(2)}) copy-start(s32[8,128]{1,0:T(8,128)} %copy-done.15) | copy-start | bytes 12292
  93.8 22.6 %copy-start.17 = (s32[8,128]{1,0:T(8,128)S(1)}, s32[8,128]{1,0:T(8,128)}, u32[]{:S(2)}) copy-start(s32[8,128]{1,0:T(8,128)} %convolution_convert_fusion.11) | copy-start | bytes 12292
  93.8 22.6 %copy-start.18 = (s32[8,128]{1,0:T(8,128)S(1)}, s32[8,128]{1,0:T(8,128)}, u32[]{:S(2)}) copy-start(s32[8,128]{1,0:T(8,128)} %convolution_convert_fusion.8) | copy-start | bytes 12292
  93.8 22.6 %copy-start.20 = (s32[8,128]{1,0:T(8,128)S(1)}, s32[8,128]{1,0:T(8,128)}, u32[]{:S(2)}) copy-start(s32[8,128]{1,0:T(8,128)} %copy-done.19) | copy-start | bytes 12292
  93.8 22.6 %copy-start.21 = (s32[256]{0:T(256)S(1)}, s32[256]{0:T(256)}, u32[]{:S(2)}) copy-start(s32[256]{0:T(256)} %eq.214) | copy-start | bytes 3076
  93.9 22.6 %copy-start.23 = (pred[8,128]{1,0:T(8,128)(4,1)S(1)}, pred[8,128]{1,0:T(8,128)(4,1)}, u32[]{:S(2)}) copy-start(pred[8,128]{1,0:T(8,128)(4,1)} %copy-done.22) | copy-start | bytes 3076
  93.9 22.6 %copy-start.25 = (pred[8,128]{1,0:T(8,128)(4,1)S(1)}, pred[8,128]{1,0:T(8,128)(4,1)}, u32[]{:S(2)}) copy-start(pred[8,128]{1,0:T(8,128)(4,1)} %copy-done.24) | copy-start | bytes 3076
  93.9 22.6 %copy-start.26 = (pred[8,128]{1,0:T(8,128)(4,1)S(1)}, pred[8,128]{1,0:T(8,128)(4,1)}, u32[]{:S(2)}) copy-start(pred[8,128]{1,0:T(8,128)(4,1)} %get-tuple-element.11) | copy-start | bytes 3076
  93.9 22.6 %copy-start.28 = (pred[8,128]{1,0:T(8,128)(4,1)S(1)}, pred[8,128]{1,0:T(8,128)(4,1)}, u32[]{:S(2)}) copy-start(pred[8,128]{1,0:T(8,128)(4,1)} %copy-done.27) | copy-start | bytes 3076
  96.9 13.7 %collective-permute-start.9 = (bf16[128,2048]{1,0:T(8,128)(2,1)}, bf16[128,2048]{1,0:T(8,128)(2,1)S(1)}, u32[]{:S(2)}, u32[]{:S(2)}) collective-permute-start(bf16[128,2048]{1,0:T(8,128)(2,1)} %collective-permute-done.7), channel_id=1, source_target_pairs={{0,8},{8,16},{16,24},{24,0},{1,9},{9,17},{17,25},{25,1},{2,10},{10... | collective-permute-start | bytes 1572872 | tf_op jit(solution)/shard_map/ppermute | solution.py:17
  112.0 18.7 %all-to-all-start.8 = ((bf16[8,32,2048]{2,1,0:T(8,128)(2,1)}), bf16[8,32,2048]{2,1,0:T(8,128)(2,1)}, u32[]{:S(2)}, u32[]{:S(2)}) async-start(bf16[8,32,2048]{2,1,0:T(8,128)(2,1)} %bitcast.221), calls=%async_computation.8 | async-start | bytes 2097152 | tf_op jit(solution)/shard_map/all_to_all | solution.py:185
  116.2 3.5 %copy-start.5 = (pred[256,128]{1,0:T(32,128)(4,1)S(1)}, pred[256,128]{1,0:T(32,128)(4,1)}, u32[]{:S(2)}) copy-start(pred[256,128]{1,0:T(32,128)(4,1)} %get-tuple-element.46) | copy-start | bytes 98308
  130.7 18.7 %all-to-all-start.6 = ((bf16[8,32,2048]{2,1,0:T(8,128)(2,1)}), bf16[8,32,2048]{2,1,0:T(8,128)(2,1)}, u32[]{:S(2)}, u32[]{:S(2)}) async-start(bf16[8,32,2048]{2,1,0:T(8,128)(2,1)} %bitcast.223), calls=%async_computation.6 | async-start | bytes 2097152 | tf_op jit(solution)/shard_map/all_to_all | solution.py:185
  134.9 3.6 %copy-start.40 = (bf16[1,2048,512]{2,1,0:T(8,128)(2,1)S(1)}, bf16[1,2048,512]{2,1,0:T(8,128)(2,1)}, u32[]{:S(2)}) copy-start(bf16[1,2048,512]{2,1,0:T(8,128)(2,1)} %param.26) | copy-start | bytes 6291460
  149.4 18.7 %all-to-all-start.9 = ((bf16[8,32,2048]{2,1,0:T(8,128)(2,1)}), bf16[8,32,2048]{2,1,0:T(8,128)(2,1)}, u32[]{:S(2)}, u32[]{:S(2)}) async-start(bf16[8,32,2048]{2,1,0:T(8,128)(2,1)} %bitcast.228), calls=%async_computation.9 | async-start | bytes 2097152 | tf_op jit(solution)/shard_map/all_to_all | solution.py:185
  153.8 3.6 %copy-start.41 = (bf16[1,2048,512]{2,1,0:T(8,128)(2,1)S(1)}, bf16[1,2048,512]{2,1,0:T(8,128)(2,1)}, u32[]{:S(2)}) copy-start(bf16[1,2048,512]{2,1,0:T(8,128)(2,1)} %param.26) | copy-start | bytes 6291460
  168.1 18.7 %all-to-all-start.7 = ((bf16[8,32,2048]{2,1,0:T(8,128)(2,1)}), bf16[8,32,2048]{2,1,0:T(8,128)(2,1)}, u32[]{:S(2)}, u32[]{:S(2)}) async-start(bf16[8,32,2048]{2,1,0:T(8,128)(2,1)} %bitcast.227), calls=%async_computation.7 | async-start | bytes 2097152 | tf_op jit(solution)/shard_map/all_to_all | solution.py:185
  175.1 17.8 %collective-permute-start.10 = (bf16[128,2048]{1,0:T(8,128)(2,1)}, bf16[128,2048]{1,0:T(8,128)(2,1)}, u32[]{:S(2)}, u32[]{:S(2)}) collective-permute-start(bf16[128,2048]{1,0:T(8,128)(2,1)} %fusion.50), channel_id=1, source_target_pairs={{0,24},{8,0},{16,8},{24,16},{1,25},{9,1},{17,9},{25,17},{2,26},{10... | collective-permute-start | bytes 1572872 | tf_op jit(solution)/shard_map/ppermute | solution.py:17
  186.9 18.7 %all-to-all-start.5 = ((bf16[8,32,2048]{2,1,0:T(8,128)(2,1)}), bf16[8,32,2048]{2,1,0:T(8,128)(2,1)}, u32[]{:S(2)}, u32[]{:S(2)}) async-start(bf16[8,32,2048]{2,1,0:T(8,128)(2,1)} %bitcast.225), calls=%async_computation.5 | async-start | bytes 2097152 | tf_op jit(solution)/shard_map/all_to_all | solution.py:185
  194.9 16.7 %collective-permute-start.11 = (bf16[128,2048]{1,0:T(8,128)(2,1)}, bf16[128,2048]{1,0:T(8,128)(2,1)}, u32[]{:S(2)}, u32[]{:S(2)}) collective-permute-start(bf16[128,2048]{1,0:T(8,128)(2,1)} %fusion.52), channel_id=1, source_target_pairs={{0,24},{8,0},{16,8},{24,16},{1,25},{9,1},{17,9},{25,17},{2,26},{10... | collective-permute-start | bytes 1572872 | tf_op jit(solution)/shard_map/ppermute | solution.py:17
  205.6 18.7 %all-to-all-start.3 = ((bf16[8,32,2048]{2,1,0:T(8,128)(2,1)}), bf16[8,32,2048]{2,1,0:T(8,128)(2,1)}, u32[]{:S(2)}, u32[]{:S(2)}) async-start(bf16[8,32,2048]{2,1,0:T(8,128)(2,1)} %bitcast.226), calls=%async_computation.3 | async-start | bytes 2097152 | tf_op jit(solution)/shard_map/all_to_all | solution.py:185
  213.6 14.5 %collective-permute-start.12 = (bf16[128,2048]{1,0:T(8,128)(2,1)}, bf16[128,2048]{1,0:T(8,128)(2,1)}, u32[]{:S(2)}, u32[]{:S(2)}) collective-permute-start(bf16[128,2048]{1,0:T(8,128)(2,1)} %fusion.54), channel_id=1, source_target_pairs={{0,24},{8,0},{16,8},{24,16},{1,25},{9,1},{17,9},{25,17},{2,26},{10... | collective-permute-start | bytes 1572872 | tf_op jit(solution)/shard_map/ppermute | solution.py:17
  218.0 10.2 %copy-start.34 = (f32[128]{0:T(128)S(1)}, f32[128]{0:T(128)}, u32[]{:S(2)}) copy-start(f32[128]{0:T(128)} %copy-done.33) | copy-start | bytes 1540
  218.0 10.2 %copy-start.37 = (f32[128]{0:T(128)S(1)}, f32[128]{0:T(128)}, u32[]{:S(2)}) copy-start(f32[128]{0:T(128)} %copy-done.36) | copy-start | bytes 1540
  224.3 3.9 %copy-start.1 = (f32[128,2048]{1,0:T(8,128)S(1)}, f32[128,2048]{1,0:T(8,128)}, u32[]{:S(2)}) copy-start(f32[128,2048]{1,0:T(8,128)} %fusion.49) | copy-start | bytes 3145732
  (2 other events, 4.1 us)

commit v2 on v1

--- a/solution.py
+++ b/solution.py
@@ -47,33 +47,39 @@
     for i in range(ny):
         if i:
             part = ring(part, "y", 1)
-        from_y = (y - i) % ny
+        from_y = jnp.where(y >= i, y - i, y - i + ny)
         found.append((from_y * nc + c, part))
         other = part
         for j in range(1, nc):
             other = ring(other, "c", 1)
-            found.append((from_y * nc + (c - j) % nc, other))
+            found.append((from_y * nc + jnp.where(c >= j, c - j, c - j + nc), other))
     return found
 
 
-def pooled(pool_in, doc_ids, w_group, pool_scale):
+def after(value, other):
+    return lax.optimization_barrier((value, other))[0]
+
+
+def tail_of(pool_in, doc_ids, lanes):
+    sp_size = lax.axis_size(SP)
+    last_doc = doc_ids[-1]
+    trailing = (doc_ids == last_doc).astype(jnp.bfloat16)
+    tail_sums = dot32(trailing[None, :], pool_in)
+    tail_count = jnp.sum(trailing.astype(jnp.float32))
+    lane = lax.broadcasted_iota(jnp.int32, (1, lanes), 1)
+    info = jnp.where(lane == 0, last_doc.astype(jnp.float32), jnp.where(lane == 1, tail_count, 0.0))
+    tail = jnp.concatenate([tail_sums, info], axis=1)
+    return jnp.broadcast_to(tail, (sp_size, tail.shape[1]))
+
+
+def pooled(pool_in, doc_ids, w_group, pool_scale, tail, before):
     tok_count, local_width = pool_in.shape
     group_width = w_group.shape[1]
     group_count = local_width // group_width
     halo = max(pool_windows)
     tp_at = lax.axis_index(TP)
     sp_size, sp_at = lax.axis_size(SP), lax.axis_index(SP)
-    before = shifted(pool_in[tok_count - halo :], SP, 1)
-    last_doc = doc_ids[-1]
-    trailing = (doc_ids == last_doc).astype(jnp.bfloat16)
-    tail_sums = dot32(trailing[None, :], pool_in)
-    tail_count = jnp.sum(trailing.astype(jnp.float32))
-    lane = lax.broadcasted_iota(jnp.int32, (1, group_width), 1)
-    info = jnp.where(lane == 0, last_doc.astype(jnp.float32), jnp.where(lane == 1, tail_count, 0.0))
-    tail = jnp.concatenate([tail_sums, info], axis=1)
-    tails = lax.all_to_all(
-        jnp.broadcast_to(tail, (sp_size, tail.shape[1])), SP, split_axis=0, concat_axis=0, tiled=True
-    )
+    tails = lax.all_to_all(tail, SP, split_axis=0, concat_axis=0, tiled=True)
     prev_doc = jnp.max(
         jnp.where(jnp.arange(sp_size) < sp_at, tails[:, local_width], -1.0)
     )
@@ -86,11 +92,15 @@
     same = (doc_ids[:, None] == doc_ids[None, :]) & (s <= t)
     local_since = jnp.sum(same.astype(jnp.float32), axis=1) - 1.0
     running = dot32(same.astype(jnp.bfloat16), pool_in)
-    table = jnp.asarray(pool_windows, dtype=jnp.int32)
-    widths = [table[tp_at * group_count + g] for g in range(group_count)]
+    widths = []
+    for g in range(group_count):
+        width = jnp.int32(pool_windows[g])
+        for i in range(g, len(pool_windows), group_count):
+            width = jnp.where(tp_at * group_count + g == i, pool_windows[i], width)
+        widths.append(width)
     recent = [
         dot32(
-            (same & (s > t - widths[g])).astype(jnp.bfloat16),
+            (same & (t - s < widths[g])).astype(jnp.bfloat16),
             pool_in[:, g * group_width : (g + 1) * group_width],
         )
         for g in range(group_count)
@@ -109,7 +119,7 @@
     mixed = []
     for g in range(group_count):
         cols = slice(g * group_width, (g + 1) * group_width)
-        early = dot32((reach & (sh > th - widths[g])).astype(jnp.bfloat16), before[:, cols])
+        early = dot32((reach & (th - sh < widths[g])).astype(jnp.bfloat16), before[:, cols])
         total = recent[g] + jnp.pad(early, ((0, tok_count - halo), (0, 0)))
         mean = total / jnp.minimum(since + 1.0, widths[g].astype(jnp.float32))
         offset = 0.5 * (mean + doc_mean[:, cols]) - pool_in[:, cols].astype(jnp.float32)
@@ -164,12 +174,14 @@
     top = route_ids.shape[1]
     capacity = 2 * row_count * top // (nz * per_plane)
     packed = jnp.concatenate([route_ids.astype(jnp.float32), route_wts], axis=1).T
-    tables = [
-        slot_tables(ring(packed, "z", r) if r else packed, top, capacity) for r in range(nz)
-    ]
+    tail = tail_of(pool_in, doc_ids, w_group.shape[1])
+    packed, w_branch = after(packed, tail), after(w_branch, tail)
+    before = shifted(pool_in[pool_in.shape[0] - max(pool_windows) :], SP, 1)
     branch_rows = gathered_rows(w_branch)
-
-    mixed = pooled(pool_in, doc_ids, w_group, pool_scale)
+    others = [ring(packed, "z", r) for r in range(1, nz)]
+
+    mixed = pooled(pool_in, doc_ids, w_group, pool_scale, tail, before)
+    first_table = slot_tables(after(packed, mixed), top, capacity)
     parts = lax.all_to_all(
         mixed.reshape(tp_size, row_count, local_width), TP, split_axis=0, concat_axis=0, tiled=True
     )
@@ -185,25 +197,37 @@
         value = lax.all_to_all(value, PLANE, split_axis=0, concat_axis=0, tiled=True)
         return value.reshape(-1, model_width)
 
+    rounds = [(r,) for r in range(nz)]
+    tables = [first_table] + [
+        slot_tables(after(other, normed), top, capacity) for other in others
+    ]
     block = normed
     arrived = []
-    for r in range(nz):
-        if r:
-            block = ring(block, "z", 1)
-        arrived.append(across(dot32(tables[r][0], block).astype(jnp.bfloat16)))
+    for members in rounds:
+        picked = []
+        for r in members:
+            if r:
+                block = ring(block, "z", 1)
+            rows = dot32(tables[r][0], block).astype(jnp.bfloat16)
+            picked.append(rows.reshape(per_plane, capacity, model_width))
+        arrived.append(across(jnp.concatenate(picked, axis=1)))
     shared = dot32(swiglu_hidden(normed, w_sh_gate, w_sh_up), w_sh_down)
 
     routed = None
-    for r in reversed(range(nz)):
-        hidden = swiglu_hidden(arrived[r], w_exp_gate[0], w_exp_up[0])
+    for members, rows in zip(reversed(rounds), reversed(arrived)):
+        hidden = swiglu_hidden(rows, w_exp_gate[0], w_exp_up[0])
         returned = across(dot32(hidden, w_exp_down[0]).astype(jnp.bfloat16))
-        both = lax.dot_general(
-            tables[r][1], returned, (((0,), (0,)), ((), ())), preferred_element_type=jnp.float32
-        )
-        partial = both[:row_count] + both[row_count:]
-        routed = partial if routed is None else partial + routed.astype(jnp.float32)
-        if r:
-            routed = ring(routed.astype(jnp.bfloat16), "z", -1)
+        returned = returned.reshape(per_plane, -1, model_width)
+        for at in reversed(range(len(members))):
+            r = members[at]
+            mine = returned[:, at * capacity : (at + 1) * capacity].reshape(-1, model_width)
+            both = lax.dot_general(
+                tables[r][1], mine, (((0,), (0,)), ((), ())), preferred_element_type=jnp.float32
+            )
+            partial = both[:row_count] + both[row_count:]
+            routed = partial if routed is None else partial + routed.astype(jnp.float32)
+            if r:
+                routed = ring(routed.astype(jnp.bfloat16), "z", -1)
     return layer_norm(alpha_mix * normed.astype(jnp.float32) + routed + shared, final_gain).astype(
         jnp.bfloat16
     )

time: 233 us -> 218 us (0.936)
  other arithmetic: 29.3 us -> 21.3 us
  waiting for transfers between devices: 69.7 us -> 63.3 us
  starting transfers between devices: 55.6 us -> 60.5 us
    all_to_all x1, waiting for transfers between devices: 3.22 us -> 0.01 us  [local(): lax.all_to_all(mixed.reshape(tp_size, row_count, local_width), TP, split_...]
    sub x4 -> x1, other arithmetic: 3.06 us -> 0.01 us  [pooled(): sh = lax.broadcasted_iota(jnp.int32, (halo, halo), 1) - halo]
    all_to_all x1, starting transfers between devices: 3.34 us -> 5.81 us  [pooled(): tails = lax.all_to_all(tail, SP, split_axis=0, concat_axis=0, tiled=True)]
  transfers between devices with their start and end apart: 23 -> 23, of which waited for: 12 -> 11; matrix products, arithmetic and copies ran while one was open for 42% -> 39% of each run, Pallas kernels for 0% -> 0%
where the time goes in v2:
time: 218 us; the launch traced here: 216 us
  matrix products  64.9 us (30%)
  waiting for transfers between devices  63.3 us (29%)
  starting transfers between devices  60.5 us (28%)
  other arithmetic  21.3 us (10%)
  local copies, waits for them, and re-layouts  5.16 us (2%)
    dot_general x23, matrix products, dot32(): return jnp.dot(a, b, preferred_element_type=jnp.float32)  43.1 us
    all_to_all x8, waiting for transfers between devices, across(): lax.all_to_all(value, PLANE, split_axis=0, concat_axis=0, tiled=True)  38.8 us
    all_to_all x8, starting transfers between devices, across(): lax.all_to_all(value, PLANE, split_axis=0, concat_axis=0, tiled=True)  34.1 us
    ppermute x12, waiting for transfers between devices, ring(): lax.ppermute(value, axis, [(i, (i + by) % length) for i in range(length)])  24.5 us
    dot_general x5, matrix products, swiglu_hidden(): jnp.dot(token_rows, gate_weight, preferred_element_type=jnp.float32)  14.8 us
    ppermute x12, starting transfers between devices, ring(): lax.ppermute(value, axis, [(i, (i + by) % length) for i in range(length)])  13.2 us
    dot_general x4, matrix products, local(): lax.dot_general(tables[r][1], mine, (((0,), (0,)), ((), ())), preferred_e...  7.05 us
    all_to_all x1, starting transfers between devices, pooled(): tails = lax.all_to_all(tail, SP, split_axis=0, concat_axis=0, tiled=True)  5.81 us
  transfers between devices with their start and end apart: 23, of which 11 were waited for; matrix products, arithmetic and copies ran while one was open for 39% of the time, Pallas kernels for 0%

profile of v2, /device:TPU:0, one launch (start us, length us, event | category | flops | bytes accessed | tf_op | source)
XLA Modules:
  0.0 216.3 jit_solution(3285424041839508660)
XLA Ops:
  0.0 1.4 slice.101
  1.4 2.0 convert_reduce_fusion.1
  4.8 1.1 fusion.214
  6.5 2.6 %collective-permute-start.2 = (bf16[256,2048]{1,0:T(8,128)(2,1)}, bf16[256,2048]{1,0:T(8,128)(2,1)}, u32[]{:S(2)}, u32[]{:S(2)}) collective-permute-start(bf16[256,2048]{1,0:T(8,128)(2,1)} %param.21), channel_id=1, source_target_pairs={{0,2},{2,0},{1,3},{3,1},{4,6},{6,4},{5,7},{7,5},{8,10},{10,8},{9,1... | collective-permute-start | bytes 3145736 | tf_op jit(solution)/shard_map/ppermute | solution.py:17
  9.7 5.8 %all-to-all-start = ((f32[8,1,384]{2,1,0:T(1,128)}), f32[8,1,384]{2,1,0:T(1,128)S(1)}, u32[]{:S(2)}, u32[]{:S(2)}) async-start(f32[8,1,384]{2,1,0:T(1,128)} %broadcast_in_dim.183), calls=%async_computation | async-start | bytes 24576 | tf_op jit(solution)/shard_map/all_to_all | solution.py:82
  16.3 3.9 %collective-permute-start = (bf16[128,256]{1,0:T(8,128)(2,1)S(1)}, bf16[128,256]{1,0:T(8,128)(2,1)S(1)}, u32[]{:S(2)}, u32[]{:S(2)}) collective-permute-start(bf16[128,256]{1,0:T(8,128)(2,1)S(1)} %slice.105), channel_id=1, source_target_pairs={{0,4},{4,8},{8,12},{12,16},{16,20},{20,24},{24,28},{1,5},{5,9},{9,... | collective-permute-start | bytes 196616 | tf_op jit(solution)/shard_map/ppermute | solution.py:23
  20.2 1.0 convert_reduce_fusion
  25.5 2.0 broadcast_minimum_fusion.1
  27.5 1.3 fusion.33
  29.0 1.3 fusion.46
  31.2 2.3 %fusion.47 = bf16[512,128]{0,1:T(8,128)(2,1)} fusion(f32[128]{0:T(128)} %get-tuple-element.61, f32[512,256]{1,0:T(8,128)} %copy-done.17, f32[128,128]{1,0:T(8,128)} %fusion.169, f32[512]{0:T(512)S(1)} %get-tuple-element.48, s32[]{:T(128)S(6)} %select_n.134, s32[512]{0:T(512)S(1)} %copy-done.6, bf16[512,256]{1,0:T(8,128)(2,1)S(1)} %copy-done.4, ...), kind=kOutput, calls=%fused_computation.46 | convolution fusion | flops 86048768 | bytes 760328 | tf_op jit(solution)/shard_map/dot_general | solution.py:39
  35.2 3.4 %all-to-all-start.1 = ((bf16[4,128,256]{2,1,0:T(8,128)(2,1)}), bf16[4,128,256]{2,1,0:T(8,128)(2,1)S(1)}, u32[]{:S(2)}, u32[]{:S(2)}) async-start(bf16[4,128,256]{2,1,0:T(8,128)(2,1)} %bitcast.227), calls=%async_computation.1 | async-start | bytes 524288 | tf_op jit(solution)/shard_map/all_to_all | solution.py:185
  39.8 1.5 collective-permute-start.4
  41.3 2.4 %collective-permute-start.6 = (f32[8,128]{1,0:T(8,128)S(1)}, f32[8,128]{1,0:T(8,128)S(1)}, u32[]{:S(2)}, u32[]{:S(2)}) collective-permute-start(f32[8,128]{1,0:T(8,128)S(1)} %maximum_bitcast_fusion), channel_id=1, source_target_pairs={{0,16},{8,24},{16,0},{24,8},{1,17},{9,25},{17,1},{25,9},{2,18},{10... | collective-permute-start | bytes 12296 | tf_op jit(solution)/shard_map/ppermute | solution.py:17
  43.6 1.5 collective-permute-start.8
  45.5 1.5 convolution_add_fusion.2
  47.1 1.6 convolution_add_fusion.1
  48.7 1.6 fusion.213
  50.6 1.0 multiply_convert_fusion.1
  54.0 2.5 %convolution_convert_fusion.7 = bf16[256,2048]{1,0:T(8,128)(2,1)} fusion(pred[256,128]{1,0:T(32,128)(4,1)S(1)} %get-tuple-element.56, bf16[128,2048]{1,0:T(8,128)(2,1)} %multiply_convert_fusion.1), kind=kOutput, calls=%fused_computation.7 | convolution fusion | flops 134742016 | bytes 1605632 | tf_op jit(solution)/shard_map/dot_general | solution.py:39
  56.5 4.2 %all-to-all-start.2 = ((bf16[8,32,2048]{2,1,0:T(8,128)(2,1)}), bf16[8,32,2048]{2,1,0:T(8,128)(2,1)}, u32[]{:S(2)}, u32[]{:S(2)}) async-start(bf16[8,32,2048]{2,1,0:T(8,128)(2,1)} %bitcast.222), calls=%async_computation.2 | async-start | bytes 2097152 | tf_op jit(solution)/shard_map/all_to_all | solution.py:197
  60.8 6.1 %collective-permute-done.5 = bf16[128,2048]{1,0:T(8,128)(2,1)} collective-permute-done((bf16[128,2048]{1,0:T(8,128)(2,1)}, bf16[128,2048]{1,0:T(8,128)(2,1)}, u32[]{:S(2)}, u32[]{:S(2)}) %collective-permute-start.5) | collective-permute-done | bytes 524320 | tf_op jit(solution)/shard_map/ppermute | solution.py:17
  66.9 2.5 %convolution_convert_fusion.5 = bf16[256,2048]{1,0:T(8,128)(2,1)} fusion(pred[256,128]{1,0:T(32,128)(4,1)S(1)} %get-tuple-element.57, bf16[128,2048]{1,0:T(8,128)(2,1)} %collective-permute-done.5), kind=kOutput, calls=%fused_computation.5 | convolution fusion | flops 134742016 | bytes 1605632 | tf_op jit(solution)/shard_map/dot_general | solution.py:39
  69.4 5.9 %all-to-all-done.2 = bf16[8,32,2048]{2,1,0:T(8,128)(2,1)} async-done(((bf16[8,32,2048]{2,1,0:T(8,128)(2,1)}), bf16[8,32,2048]{2,1,0:T(8,128)(2,1)}, u32[]{:S(2)}, u32[]{:S(2)}) %all-to-all-start.2) | async-done | bytes 1048608 | tf_op jit(solution)/shard_map/all_to_all | solution.py:197
  75.2 4.2 %all-to-all-start.4 = ((bf16[8,32,2048]{2,1,0:T(8,128)(2,1)}), bf16[8,32,2048]{2,1,0:T(8,128)(2,1)}, u32[]{:S(2)}, u32[]{:S(2)}) async-start(bf16[8,32,2048]{2,1,0:T(8,128)(2,1)} %bitcast.220), calls=%async_computation.4 | async-start | bytes 2097152 | tf_op jit(solution)/shard_map/all_to_all | solution.py:197
  79.5 1.7 collective-permute-done.7
  81.2 14.5 %collective-permute-done.9 = bf16[128,2048]{1,0:T(8,128)(2,1)S(1)} collective-permute-done((bf16[128,2048]{1,0:T(8,128)(2,1)}, bf16[128,2048]{1,0:T(8,128)(2,1)S(1)}, u32[]{:S(2)}, u32[]{:S(2)}) %collective-permute-start.9) | collective-permute-done | bytes 524320 | tf_op jit(solution)/shard_map/ppermute | solution.py:17
  95.8 1.4 convolution_convert_fusion.1
  97.2 4.2 %all-to-all-start.8 = ((bf16[8,32,2048]{2,1,0:T(8,128)(2,1)}), bf16[8,32,2048]{2,1,0:T(8,128)(2,1)}, u32[]{:S(2)}, u32[]{:S(2)}) async-start(bf16[8,32,2048]{2,1,0:T(8,128)(2,1)} %bitcast.219), calls=%async_computation.8 | async-start | bytes 2097152 | tf_op jit(solution)/shard_map/all_to_all | solution.py:197
  101.5 1.0 reduce-precision_convert_fusion.3
  102.6 2.2 %fusion.215 = f32[128,512]{1,0:T(8,128)S(1)} fusion(bf16[128,2048]{1,0:T(8,128)(2,1)} %multiply_convert_fusion.1, bf16[2048,512]{1,0:T(8,128)(2,1)} %param.28), kind=kOutput, calls=%fused_computation.260 | convolution fusion | flops 268435456 | bytes 2883584 | tf_op jit(solution)/shard_map/dot_general | solution.py:33
  104.8 2.4 %convolution_convert_fusion.3 = bf16[256,2048]{1,0:T(8,128)(2,1)} fusion(pred[256,128]{1,0:T(32,128)(4,1)S(1)} %copy-done.5, bf16[128,2048]{1,0:T(8,128)(2,1)} %collective-permute-done.7), kind=kOutput, calls=%fused_computation.3 | convolution fusion | flops 134742016 | bytes 1605632 | tf_op jit(solution)/shard_map/dot_general | solution.py:39
  107.2 8.7 %all-to-all-done.8 = bf16[8,32,2048]{2,1,0:T(8,128)(2,1)} async-done(((bf16[8,32,2048]{2,1,0:T(8,128)(2,1)}), bf16[8,32,2048]{2,1,0:T(8,128)(2,1)}, u32[]{:S(2)}, u32[]{:S(2)}) %all-to-all-start.8) | async-done | bytes 1048608 | tf_op jit(solution)/shard_map/all_to_all | solution.py:197
  115.9 4.2 %all-to-all-start.6 = ((bf16[8,32,2048]{2,1,0:T(8,128)(2,1)}), bf16[8,32,2048]{2,1,0:T(8,128)(2,1)}, u32[]{:S(2)}, u32[]{:S(2)}) async-start(bf16[8,32,2048]{2,1,0:T(8,128)(2,1)} %bitcast.221), calls=%async_computation.6 | async-start | bytes 2097152 | tf_op jit(solution)/shard_map/all_to_all | solution.py:197
  120.2 3.6 %fusion.19 = f32[256,512]{1,0:T(8,128)} fusion(bf16[256,2048]{1,0:T(8,128)(2,1)} %bitcast.18, bf16[1,2048,512]{2,1,0:T(8,128)(2,1)} %param.25), kind=kOutput, calls=%fused_computation.30 | convolution fusion | flops 536870912 | bytes 3670016 | tf_op jit(solution)/shard_map/dot_general | solution.py:33
  123.7 2.7 %fusion.13 = f32[256,512]{1,0:T(8,128)} fusion(bf16[256,2048]{1,0:T(8,128)(2,1)} %bitcast.42, bf16[1,2048,512]{2,1,0:T(8,128)(2,1)S(1)} %copy-done.15), kind=kOutput, calls=%fused_computation.24 | convolution fusion | flops 536870912 | bytes 3670016 | tf_op jit(solution)/shard_map/dot_general | solution.py:33
  126.5 4.3 %convolution_convert_fusion = bf16[256,2048]{1,0:T(8,128)(2,1)} fusion(bf16[1,512,2048]{2,1,0:T(8,128)(2,1)S(1)} %copy-done, bf16[256,2048]{1,0:T(8,128)(2,1)} %bitcast.42, bf16[1,2048,512]{2,1,0:T(8,128)(2,1)} %param.26, f32[256,512]{1,0:T(8,128)} %fusion.13), kind=kOutput, calls=%fused_computation | convolution fusion | flops 1075052544 | bytes 6815744 | tf_op jit(solution)/shard_map/dot_general | solution.py:39
  130.8 3.8 %all-to-all-done.6 = bf16[8,32,2048]{2,1,0:T(8,128)(2,1)} async-done(((bf16[8,32,2048]{2,1,0:T(8,128)(2,1)}), bf16[8,32,2048]{2,1,0:T(8,128)(2,1)}, u32[]{:S(2)}, u32[]{:S(2)}) %all-to-all-start.6) | async-done | bytes 1048608 | tf_op jit(solution)/shard_map/all_to_all | solution.py:197
  134.6 4.4 %all-to-all-start.9 = ((bf16[8,32,2048]{2,1,0:T(8,128)(2,1)}), bf16[8,32,2048]{2,1,0:T(8,128)(2,1)}, u32[]{:S(2)}, u32[]{:S(2)}) async-start(bf16[8,32,2048]{2,1,0:T(8,128)(2,1)} %bitcast.226), calls=%async_computation.9 | async-start | bytes 2097152 | tf_op jit(solution)/shard_map/all_to_all | solution.py:197
  139.1 3.6 %fusion.17 = f32[256,512]{1,0:T(8,128)} fusion(bf16[256,2048]{1,0:T(8,128)(2,1)} %bitcast.28, bf16[1,2048,512]{2,1,0:T(8,128)(2,1)} %param.25), kind=kOutput, calls=%fused_computation.28 | convolution fusion | flops 536870912 | bytes 3670016 | tf_op jit(solution)/shard_map/dot_general | solution.py:33
  142.6 2.7 %fusion.15 = f32[256,512]{1,0:T(8,128)} fusion(bf16[256,2048]{1,0:T(8,128)(2,1)} %bitcast.35, bf16[1,2048,512]{2,1,0:T(8,128)(2,1)S(1)} %copy-done.16), kind=kOutput, calls=%fused_computation.26 | convolution fusion | flops 536870912 | bytes 3670016 | tf_op jit(solution)/shard_map/dot_general | solution.py:33
  145.4 4.3 %convolution_convert_fusion.2 = bf16[256,2048]{1,0:T(8,128)(2,1)} fusion(bf16[1,512,2048]{2,1,0:T(8,128)(2,1)S(1)} %copy-done, bf16[256,2048]{1,0:T(8,128)(2,1)} %bitcast.35, bf16[1,2048,512]{2,1,0:T(8,128)(2,1)} %param.26, f32[256,512]{1,0:T(8,128)} %fusion.15), kind=kOutput, calls=%fused_computation.2 | convolution fusion | flops 1075052544 | bytes 6815744 | tf_op jit(solution)/shard_map/dot_general | solution.py:39
  149.7 3.7 %all-to-all-done.9 = bf16[8,32,2048]{2,1,0:T(8,128)(2,1)} async-done(((bf16[8,32,2048]{2,1,0:T(8,128)(2,1)}), bf16[8,32,2048]{2,1,0:T(8,128)(2,1)}, u32[]{:S(2)}, u32[]{:S(2)}) %all-to-all-start.9) | async-done | bytes 1048608 | tf_op jit(solution)/shard_map/all_to_all | solution.py:197
  153.4 4.2 %all-to-all-start.7 = ((bf16[8,32,2048]{2,1,0:T(8,128)(2,1)}), bf16[8,32,2048]{2,1,0:T(8,128)(2,1)}, u32[]{:S(2)}, u32[]{:S(2)}) async-start(bf16[8,32,2048]{2,1,0:T(8,128)(2,1)} %bitcast.225), calls=%async_computation.7 | async-start | bytes 2097152 | tf_op jit(solution)/shard_map/all_to_all | solution.py:197
  157.6 1.8 fusion.131
  160.3 1.1 collective-permute-start.10
  161.4 4.3 %convolution_convert_fusion.4 = bf16[256,2048]{1,0:T(8,128)(2,1)} fusion(bf16[1,512,2048]{2,1,0:T(8,128)(2,1)S(1)} %copy-done, bf16[256,2048]{1,0:T(8,128)(2,1)} %bitcast.28, bf16[1,2048,512]{2,1,0:T(8,128)(2,1)} %param.26, f32[256,512]{1,0:T(8,128)} %fusion.17), kind=kOutput, calls=%fused_computation.4 | convolution fusion | flops 1075052544 | bytes 6815744 | tf_op jit(solution)/shard_map/dot_general | solution.py:39
  165.8 6.3 %all-to-all-done.7 = bf16[8,32,2048]{2,1,0:T(8,128)(2,1)} async-done(((bf16[8,32,2048]{2,1,0:T(8,128)(2,1)}), bf16[8,32,2048]{2,1,0:T(8,128)(2,1)}, u32[]{:S(2)}, u32[]{:S(2)}) %all-to-all-start.7) | async-done | bytes 1048608 | tf_op jit(solution)/shard_map/all_to_all | solution.py:197
  172.1 4.2 %all-to-all-start.5 = ((bf16[8,32,2048]{2,1,0:T(8,128)(2,1)}), bf16[8,32,2048]{2,1,0:T(8,128)(2,1)}, u32[]{:S(2)}, u32[]{:S(2)}) async-start(bf16[8,32,2048]{2,1,0:T(8,128)(2,1)} %bitcast.223), calls=%async_computation.5 | async-start | bytes 2097152 | tf_op jit(solution)/shard_map/all_to_all | solution.py:197
  176.3 1.8 fusion.127
  178.1 2.0 fusion.52
  180.1 1.1 collective-permute-start.11
  181.3 4.3 %convolution_convert_fusion.6 = bf16[256,2048]{1,0:T(8,128)(2,1)} fusion(bf16[1,512,2048]{2,1,0:T(8,128)(2,1)S(1)} %copy-done, bf16[256,2048]{1,0:T(8,128)(2,1)} %bitcast.18, bf16[1,2048,512]{2,1,0:T(8,128)(2,1)} %param.26, f32[256,512]{1,0:T(8,128)} %fusion.19), kind=kOutput, calls=%fused_computation.6 | convolution fusion | flops 1075052544 | bytes 6815744 | tf_op jit(solution)/shard_map/dot_general | solution.py:39
  185.6 5.2 %all-to-all-done.5 = bf16[8,32,2048]{2,1,0:T(8,128)(2,1)} async-done(((bf16[8,32,2048]{2,1,0:T(8,128)(2,1)}), bf16[8,32,2048]{2,1,0:T(8,128)(2,1)}, u32[]{:S(2)}, u32[]{:S(2)}) %all-to-all-start.5) | async-done | bytes 1048608 | tf_op jit(solution)/shard_map/all_to_all | solution.py:197
  190.8 4.2 %all-to-all-start.3 = ((bf16[8,32,2048]{2,1,0:T(8,128)(2,1)}), bf16[8,32,2048]{2,1,0:T(8,128)(2,1)}, u32[]{:S(2)}, u32[]{:S(2)}) async-start(bf16[8,32,2048]{2,1,0:T(8,128)(2,1)} %bitcast.224), calls=%async_computation.3 | async-start | bytes 2097152 | tf_op jit(solution)/shard_map/all_to_all | solution.py:197
  195.1 1.8 fusion.123
  196.8 2.1 fusion.54
  198.9 1.1 collective-permute-start.12
  200.0 4.3 %fusion.49 = f32[128,2048]{1,0:T(8,128)} fusion(bf16[512,2048]{1,0:T(8,128)(2,1)} %param.30, bf16[128,2048]{1,0:T(8,128)(2,1)} %multiply_convert_fusion.1, bf16[2048,512]{1,0:T(8,128)(2,1)} %param.29, f32[128,512]{1,0:T(8,128)S(1)} %fusion.215), kind=kOutput, calls=%fused_computation.48 | convolution fusion | flops 537264128 | bytes 6029312 | tf_op jit(solution)/shard_map/dot_general | solution.py:39
  204.3 5.2 %all-to-all-done.3 = bf16[8,32,2048]{2,1,0:T(8,128)(2,1)} async-done(((bf16[8,32,2048]{2,1,0:T(8,128)(2,1)}), bf16[8,32,2048]{2,1,0:T(8,128)(2,1)}, u32[]{:S(2)}, u32[]{:S(2)}) %all-to-all-start.3) | async-done | bytes 1048608 | tf_op jit(solution)/shard_map/all_to_all | solution.py:197
  209.5 1.8 fusion.119
  211.3 2.1 collective-permute-done.12
  213.4 1.5 fusion.207
  215.2 1.0 multiply_convert_fusion
  (98 shorter events, 15.2 us)
Async XLA Ops:
  0.0 126.5 %copy-start = (bf16[1,512,2048]{2,1,0:T(8,128)(2,1)S(1)}, bf16[1,512,2048]{2,1,0:T(8,128)(2,1)}, u32[]{:S(2)}) copy-start(bf16[1,512,2048]{2,1,0:T(8,128)(2,1)} %param.27) | copy-start | bytes 6291460
  0.0 29.0 %copy-start.6 = (s32[512]{0:T(512)S(1)}, s32[512]{0:T(512)}, u32[]{:S(2)}) copy-start(s32[512]{0:T(512)} %param.18) | copy-start | bytes 6148
  0.0 29.0 %copy-start.4 = (bf16[512,256]{1,0:T(8,128)(2,1)S(1)}, bf16[512,256]{1,0:T(8,128)(2,1)}, u32[]{:S(2)}) copy-start(bf16[512,256]{1,0:T(8,128)(2,1)} %param.17) | copy-start | bytes 786436
  5.9 39.6 %collective-permute-start.1 = (bf16[256,2048]{1,0:T(8,128)(2,1)}, bf16[256,2048]{1,0:T(8,128)(2,1)}, u32[]{:S(2)}, u32[]{:S(2)}) collective-permute-start(bf16[256,2048]{1,0:T(8,128)(2,1)} %param.21), channel_id=1, source_target_pairs={{0,1},{1,0},{2,3},{3,2},{4,5},{5,4},{6,7},{7,6},{8,9},{9,8},{10,11... | collective-permute-start | bytes 3145736 | tf_op jit(solution)/shard_map/ppermute | solution.py:17
  6.5 32.2 %collective-permute-start.2 = (bf16[256,2048]{1,0:T(8,128)(2,1)}, bf16[256,2048]{1,0:T(8,128)(2,1)}, u32[]{:S(2)}, u32[]{:S(2)}) collective-permute-start(bf16[256,2048]{1,0:T(8,128)(2,1)} %param.21), channel_id=1, source_target_pairs={{0,2},{2,0},{1,3},{3,1},{4,6},{6,4},{5,7},{7,5},{8,10},{10,8},{9,1... | collective-permute-start | bytes 3145736 | tf_op jit(solution)/shard_map/ppermute | solution.py:17
  9.7 13.6 %all-to-all-start = ((f32[8,1,384]{2,1,0:T(1,128)}), f32[8,1,384]{2,1,0:T(1,128)S(1)}, u32[]{:S(2)}, u32[]{:S(2)}) async-start(f32[8,1,384]{2,1,0:T(1,128)} %broadcast_in_dim.183), calls=%async_computation | async-start | bytes 24576 | tf_op jit(solution)/shard_map/all_to_all | solution.py:82
  16.3 12.5 %collective-permute-start = (bf16[128,256]{1,0:T(8,128)(2,1)S(1)}, bf16[128,256]{1,0:T(8,128)(2,1)S(1)}, u32[]{:S(2)}, u32[]{:S(2)}) collective-permute-start(bf16[128,256]{1,0:T(8,128)(2,1)S(1)} %slice.105), channel_id=1, source_target_pairs={{0,4},{4,8},{8,12},{12,16},{16,20},{20,24},{24,28},{1,5},{5,9},{9,... | collective-permute-start | bytes 196616 | tf_op jit(solution)/shard_map/ppermute | solution.py:23
  28.8 2.4 %copy-start.17 = (f32[512,256]{1,0:T(8,128)}, f32[512,256]{1,0:T(8,128)S(1)}, u32[]{:S(2)}) copy-start(f32[512,256]{1,0:T(8,128)S(1)} %fusion.33) | copy-start | bytes 1572868
  31.2 13.9 %copy-start.11 = (bf16[2048]{0:T(1024)(128)(2,1)S(1)}, bf16[2048]{0:T(1024)(128)(2,1)}, u32[]{:S(2)}) copy-start(bf16[2048]{0:T(1024)(128)(2,1)} %param.22) | copy-start | bytes 12292
  31.2 14.0 %copy-start.2 = (bf16[256,2048]{1,0:T(8,128)(2,1)S(1)}, bf16[256,2048]{1,0:T(8,128)(2,1)}, u32[]{:S(2)}) copy-start(bf16[256,2048]{1,0:T(8,128)(2,1)} %param.21) | copy-start | bytes 3145732
  35.2 10.0 %all-to-all-start.1 = ((bf16[4,128,256]{2,1,0:T(8,128)(2,1)}), bf16[4,128,256]{2,1,0:T(8,128)(2,1)S(1)}, u32[]{:S(2)}, u32[]{:S(2)}) async-start(bf16[4,128,256]{2,1,0:T(8,128)(2,1)} %bitcast.227), calls=%async_computation.1 | async-start | bytes 524288 | tf_op jit(solution)/shard_map/all_to_all | solution.py:185
  38.7 10.0 %collective-permute-start.3 = (bf16[256,2048]{1,0:T(8,128)(2,1)}, bf16[256,2048]{1,0:T(8,128)(2,1)}, u32[]{:S(2)}, u32[]{:S(2)}) collective-permute-start(bf16[256,2048]{1,0:T(8,128)(2,1)} %collective-permute-done.2), channel_id=1, source_target_pairs={{0,1},{1,0},{2,3},{3,2},{4,5},{5,4},{6,7},{7,6},{8,9},{9,8},{10,11... | collective-permute-start | bytes 3145736 | tf_op jit(solution)/shard_map/ppermute | solution.py:17
  39.8 12.7 %collective-permute-start.4 = (f32[8,128]{1,0:T(8,128)S(1)}, f32[8,128]{1,0:T(8,128)S(1)}, u32[]{:S(2)}, u32[]{:S(2)}) collective-permute-start(f32[8,128]{1,0:T(8,128)S(1)} %maximum_bitcast_fusion), channel_id=1, source_target_pairs={{0,8},{8,16},{16,24},{24,0},{1,9},{9,17},{17,25},{25,1},{2,10},{10... | collective-permute-start | bytes 12296 | tf_op jit(solution)/shard_map/ppermute | solution.py:17
  41.3 11.3 %collective-permute-start.6 = (f32[8,128]{1,0:T(8,128)S(1)}, f32[8,128]{1,0:T(8,128)S(1)}, u32[]{:S(2)}, u32[]{:S(2)}) collective-permute-start(f32[8,128]{1,0:T(8,128)S(1)} %maximum_bitcast_fusion), channel_id=1, source_target_pairs={{0,16},{8,24},{16,0},{24,8},{1,17},{9,25},{17,1},{25,9},{2,18},{10... | collective-permute-start | bytes 12296 | tf_op jit(solution)/shard_map/ppermute | solution.py:17
  43.6 8.9 %collective-permute-start.8 = (f32[8,128]{1,0:T(8,128)S(1)}, f32[8,128]{1,0:T(8,128)S(1)}, u32[]{:S(2)}, u32[]{:S(2)}) collective-permute-start(f32[8,128]{1,0:T(8,128)S(1)} %maximum_bitcast_fusion), channel_id=1, source_target_pairs={{0,24},{8,0},{16,8},{24,16},{1,25},{9,1},{17,9},{25,17},{2,26},{10... | collective-permute-start | bytes 12296 | tf_op jit(solution)/shard_map/ppermute | solution.py:17
  45.2 8.0 %copy-start.7 = (s32[256]{0:T(256)}, s32[256]{0:T(256)S(1)}, u32[]{:S(2)}) copy-start(s32[256]{0:T(256)S(1)} %eq.235) | copy-start | bytes 3076
  47.1 1.6 copy-start.3
  50.4 2.2 %copy-start.9 = (f32[128]{0:T(128)}, f32[128]{0:T(128)S(1)}, u32[]{:S(2)}) copy-start(f32[128]{0:T(128)S(1)} %broadcast_multiply_fusion.1) | copy-start | bytes 1540
  50.6 1.9 copy-start.13
  51.6 15.2 %collective-permute-start.5 = (bf16[128,2048]{1,0:T(8,128)(2,1)}, bf16[128,2048]{1,0:T(8,128)(2,1)}, u32[]{:S(2)}, u32[]{:S(2)}) collective-permute-start(bf16[128,2048]{1,0:T(8,128)(2,1)} %multiply_convert_fusion.1), channel_id=1, source_target_pairs={{0,8},{8,16},{16,24},{24,0},{1,9},{9,17},{17,25},{25,1},{2,10},{10... | collective-permute-start | bytes 1572872 | tf_op jit(solution)/shard_map/ppermute | solution.py:17
  56.5 18.7 %all-to-all-start.2 = ((bf16[8,32,2048]{2,1,0:T(8,128)(2,1)}), bf16[8,32,2048]{2,1,0:T(8,128)(2,1)}, u32[]{:S(2)}, u32[]{:S(2)}) async-start(bf16[8,32,2048]{2,1,0:T(8,128)(2,1)} %bitcast.222), calls=%async_computation.2 | async-start | bytes 2097152 | tf_op jit(solution)/shard_map/all_to_all | solution.py:197
  66.9 14.4 %collective-permute-start.7 = (bf16[128,2048]{1,0:T(8,128)(2,1)}, bf16[128,2048]{1,0:T(8,128)(2,1)}, u32[]{:S(2)}, u32[]{:S(2)}) collective-permute-start(bf16[128,2048]{1,0:T(8,128)(2,1)} %collective-permute-done.5), channel_id=1, source_target_pairs={{0,8},{8,16},{16,24},{24,0},{1,9},{9,17},{17,25},{25,1},{2,10},{10... | collective-permute-start | bytes 1572872 | tf_op jit(solution)/shard_map/ppermute | solution.py:17
  75.2 21.9 %all-to-all-start.4 = ((bf16[8,32,2048]{2,1,0:T(8,128)(2,1)}), bf16[8,32,2048]{2,1,0:T(8,128)(2,1)}, u32[]{:S(2)}, u32[]{:S(2)}) async-start(bf16[8,32,2048]{2,1,0:T(8,128)(2,1)} %bitcast.220), calls=%async_computation.4 | async-start | bytes 2097152 | tf_op jit(solution)/shard_map/all_to_all | solution.py:197
  79.5 21.9 %copy-start.12 = (bf16[2048]{0:T(1024)(128)(2,1)S(1)}, bf16[2048]{0:T(1024)(128)(2,1)}, u32[]{:S(2)}) copy-start(bf16[2048]{0:T(1024)(128)(2,1)} %param.31) | copy-start | bytes 12292
  79.5 22.0 %copy-start.8 = (s32[256]{0:T(256)S(1)}, s32[256]{0:T(256)}, u32[]{:S(2)}) copy-start(s32[256]{0:T(256)} %copy-done.7) | copy-start | bytes 3076
  81.2 14.5 %collective-permute-start.9 = (bf16[128,2048]{1,0:T(8,128)(2,1)}, bf16[128,2048]{1,0:T(8,128)(2,1)S(1)}, u32[]{:S(2)}, u32[]{:S(2)}) collective-permute-start(bf16[128,2048]{1,0:T(8,128)(2,1)} %collective-permute-done.7), channel_id=1, source_target_pairs={{0,8},{8,16},{16,24},{24,0},{1,9},{9,17},{17,25},{25,1},{2,10},{10... | collective-permute-start | bytes 1572872 | tf_op jit(solution)/shard_map/ppermute | solution.py:17
  97.2 18.7 %all-to-all-start.8 = ((bf16[8,32,2048]{2,1,0:T(8,128)(2,1)}), bf16[8,32,2048]{2,1,0:T(8,128)(2,1)}, u32[]{:S(2)}, u32[]{:S(2)}) async-start(bf16[8,32,2048]{2,1,0:T(8,128)(2,1)} %bitcast.219), calls=%async_computation.8 | async-start | bytes 2097152 | tf_op jit(solution)/shard_map/all_to_all | solution.py:197
  101.4 3.3 %copy-start.5 = (pred[256,128]{1,0:T(32,128)(4,1)S(1)}, pred[256,128]{1,0:T(32,128)(4,1)}, u32[]{:S(2)}) copy-start(pred[256,128]{1,0:T(32,128)(4,1)} %get-tuple-element.58) | copy-start | bytes 98308
  115.9 18.7 %all-to-all-start.6 = ((bf16[8,32,2048]{2,1,0:T(8,128)(2,1)}), bf16[8,32,2048]{2,1,0:T(8,128)(2,1)}, u32[]{:S(2)}, u32[]{:S(2)}) async-start(bf16[8,32,2048]{2,1,0:T(8,128)(2,1)} %bitcast.221), calls=%async_computation.6 | async-start | bytes 2097152 | tf_op jit(solution)/shard_map/all_to_all | solution.py:197
  120.2 3.6 %copy-start.15 = (bf16[1,2048,512]{2,1,0:T(8,128)(2,1)S(1)}, bf16[1,2048,512]{2,1,0:T(8,128)(2,1)}, u32[]{:S(2)}) copy-start(bf16[1,2048,512]{2,1,0:T(8,128)(2,1)} %param.25) | copy-start | bytes 6291460
  134.6 18.7 %all-to-all-start.9 = ((bf16[8,32,2048]{2,1,0:T(8,128)(2,1)}), bf16[8,32,2048]{2,1,0:T(8,128)(2,1)}, u32[]{:S(2)}, u32[]{:S(2)}) async-start(bf16[8,32,2048]{2,1,0:T(8,128)(2,1)} %bitcast.226), calls=%async_computation.9 | async-start | bytes 2097152 | tf_op jit(solution)/shard_map/all_to_all | solution.py:197
  139.1 3.6 %copy-start.16 = (bf16[1,2048,512]{2,1,0:T(8,128)(2,1)S(1)}, bf16[1,2048,512]{2,1,0:T(8,128)(2,1)}, u32[]{:S(2)}) copy-start(bf16[1,2048,512]{2,1,0:T(8,128)(2,1)} %param.25) | copy-start | bytes 6291460
  153.4 18.7 %all-to-all-start.7 = ((bf16[8,32,2048]{2,1,0:T(8,128)(2,1)}), bf16[8,32,2048]{2,1,0:T(8,128)(2,1)}, u32[]{:S(2)}, u32[]{:S(2)}) async-start(bf16[8,32,2048]{2,1,0:T(8,128)(2,1)} %bitcast.225), calls=%async_computation.7 | async-start | bytes 2097152 | tf_op jit(solution)/shard_map/all_to_all | solution.py:197
  160.3 17.8 %collective-permute-start.10 = (bf16[128,2048]{1,0:T(8,128)(2,1)}, bf16[128,2048]{1,0:T(8,128)(2,1)}, u32[]{:S(2)}, u32[]{:S(2)}) collective-permute-start(bf16[128,2048]{1,0:T(8,128)(2,1)} %fusion.50), channel_id=1, source_target_pairs={{0,24},{8,0},{16,8},{24,16},{1,25},{9,1},{17,9},{25,17},{2,26},{10... | collective-permute-start | bytes 1572872 | tf_op jit(solution)/shard_map/ppermute | solution.py:17
  172.1 18.7 %all-to-all-start.5 = ((bf16[8,32,2048]{2,1,0:T(8,128)(2,1)}), bf16[8,32,2048]{2,1,0:T(8,128)(2,1)}, u32[]{:S(2)}, u32[]{:S(2)}) async-start(bf16[8,32,2048]{2,1,0:T(8,128)(2,1)} %bitcast.223), calls=%async_computation.5 | async-start | bytes 2097152 | tf_op jit(solution)/shard_map/all_to_all | solution.py:197
  180.1 16.7 %collective-permute-start.11 = (bf16[128,2048]{1,0:T(8,128)(2,1)}, bf16[128,2048]{1,0:T(8,128)(2,1)}, u32[]{:S(2)}, u32[]{:S(2)}) collective-permute-start(bf16[128,2048]{1,0:T(8,128)(2,1)} %fusion.52), channel_id=1, source_target_pairs={{0,24},{8,0},{16,8},{24,16},{1,25},{9,1},{17,9},{25,17},{2,26},{10... | collective-permute-start | bytes 1572872 | tf_op jit(solution)/shard_map/ppermute | solution.py:17
  190.8 18.7 %all-to-all-start.3 = ((bf16[8,32,2048]{2,1,0:T(8,128)(2,1)}), bf16[8,32,2048]{2,1,0:T(8,128)(2,1)}, u32[]{:S(2)}, u32[]{:S(2)}) async-start(bf16[8,32,2048]{2,1,0:T(8,128)(2,1)} %bitcast.224), calls=%async_computation.3 | async-start | bytes 2097152 | tf_op jit(solution)/shard_map/all_to_all | solution.py:197
  198.9 14.5 %collective-permute-start.12 = (bf16[128,2048]{1,0:T(8,128)(2,1)}, bf16[128,2048]{1,0:T(8,128)(2,1)}, u32[]{:S(2)}, u32[]{:S(2)}) collective-permute-start(bf16[128,2048]{1,0:T(8,128)(2,1)} %fusion.54), channel_id=1, source_target_pairs={{0,24},{8,0},{16,8},{24,16},{1,25},{9,1},{17,9},{25,17},{2,26},{10... | collective-permute-start | bytes 1572872 | tf_op jit(solution)/shard_map/ppermute | solution.py:17
  204.3 9.1 %copy-start.10 = (f32[128]{0:T(128)S(1)}, f32[128]{0:T(128)}, u32[]{:S(2)}) copy-start(f32[128]{0:T(128)} %copy-done.9) | copy-start | bytes 1540
  204.3 9.1 %copy-start.14 = (f32[128]{0:T(128)S(1)}, f32[128]{0:T(128)}, u32[]{:S(2)}) copy-start(f32[128]{0:T(128)} %copy-done.13) | copy-start | bytes 1540
  209.5 3.9 %copy-start.1 = (f32[128,2048]{1,0:T(8,128)S(1)}, f32[128,2048]{1,0:T(8,128)}, u32[]{:S(2)}) copy-start(f32[128,2048]{1,0:T(8,128)} %fusion.49) | copy-start | bytes 3145732
